TPU v7x, 32 devices: a whole 2x2x4 slice. The times are simulated.
32 devices in a mesh: row: 16 (over z, y, x), col: 2 (over core).
Axes of the slice: x: 2, y: 2, z: 4, core: 2. Of those that a mesh axis runs over, the one named last changes fastest.
Arguments:
- tokens: bfloat16 [2, 6144, 2048], P('col', 'row'), may hold values from -6 to 6
- norm_gain: bfloat16 [2048], replicated, may hold values from 0.099609375 to 1.8984375
- in_weight: bfloat16 [2048, 512], P('row', 'col'), may hold values from -0.125 to 0.125
- out_weight: bfloat16 [512, 2048], P('col', 'row'), may hold values from -0.25 to 0.25
Outputs:
- mixed: bfloat16 [2, 6144, 2048], P('col', 'row')
All inputs are finite; a program needn't handle non-finite values.
Results may differ from a plain program's by a relative error of at most 0.013.
Values may be sent and summed in bfloat16 or wider, within the bound.
No kernel may reach another device: no remote copies, remote signals or barrier semaphores. Data moves between devices by JAX's collectives and lax.ppermute only.
A program may use at most 64 MiB of HBM per device.

v0:
```python
import math

import jax
import jax.numpy as jnp
import numpy as np
from jax import lax
from jax.experimental import pallas as pl
from jax.experimental.pallas import tpu as pltpu
from jax.sharding import PartitionSpec as P


GS = 64
EPS = 1e-06
BF = jnp.bfloat16
F32 = jnp.float32


def angles(left, right, modulus):
    product = np.outer(np.asarray(left, np.int64), np.asarray(right, np.int64)) % modulus
    radians = product.astype(np.float64) * (2.0 * math.pi / modulus)
    return np.cos(radians), np.sin(radians)


def group_tables():
    cos, sin = angles(np.arange(GS), np.arange(GS), GS)
    half = GS // 2
    split = np.concatenate([cos[:, : half + 1], sin[:, 1:half]], axis=1)
    join = np.zeros((GS, GS))
    for j in range(half + 1):
        join[j, j] = 1.0
    for j in range(1, half):
        join[half + j, j] = -1.0
        join[j, GS - j] = 1.0
        join[half + j, GS - j] = 1.0
    return split, join


def spread_half(shard, peers):
    near = peers // 2
    other = lax.ppermute(shard, "row", [(i, i ^ near) for i in range(peers)])
    upper = lax.axis_index("row") >= near
    both = jnp.stack([jnp.where(upper, other, shard), jnp.where(upper, shard, other)])
    copies = jnp.broadcast_to(both[None], (near,) + both.shape)
    groups = [list(range(near)), list(range(near, peers))]
    got = lax.all_to_all(copies, "row", split_axis=0, concat_axis=0, tiled=True, axis_index_groups=groups)
    return got.transpose(1, 0, *range(2, got.ndim)).reshape((peers,) + shard.shape)


def column_parts(own, cols):
    if cols == 2:
        return [own, lax.ppermute(own, "col", [(0, 1), (1, 0)])]
    got = lax.all_gather(own, "col", axis=0, tiled=False)
    return [got[i] for i in range(cols)]


def dot(a, b, dims=((1,), (0,))):
    return lax.dot_general(a, b, (dims, ((), ())), preferred_element_type=F32)


def body_general(tokens, norm_gain, in_weight, out_weight):
    peers = lax.axis_size("row")
    cols = lax.axis_size("col")
    rows = tokens.shape[1]
    length = rows * peers
    channels = in_weight.shape[1] * cols
    narrow = channels // peers
    inner = rows // peers

    in_own = spread_half(in_weight, peers)
    in_own = in_own.reshape(-1, in_weight.shape[1])
    in_parts = column_parts(in_own, cols)
    out_own = spread_half(out_weight, peers)
    out_own = out_own.transpose(1, 0, 2).reshape(out_weight.shape[0], -1)
    out_parts = column_parts(out_own, cols)

    own_rows = tokens[0].astype(F32)
    inverse_rms = lax.rsqrt(jnp.mean(own_rows * own_rows, axis=-1, keepdims=True) + EPS)
    normed = (own_rows * inverse_rms * norm_gain.astype(F32)).astype(BF)
    projected = jnp.concatenate([dot(normed, part).astype(BF) for part in in_parts], axis=1)

    split, join = group_tables()
    groups = channels // GS
    split_all = jnp.asarray(np.kron(np.eye(groups), split.T), BF)
    join_all = jnp.asarray(np.kron(np.eye(groups), join), BF)
    sums = dot(split_all, projected, ((1,), (1,))).astype(BF)

    got = lax.all_to_all(sums.reshape(peers, narrow, rows), "row", split_axis=0, concat_axis=0, tiled=True)
    small_cos, small_sin = angles(np.arange(peers), np.arange(peers), peers)
    first = jnp.asarray(np.kron(np.concatenate([small_cos, -small_sin]), np.eye(narrow)), BF)
    stage = dot(first, got.reshape(channels, rows)).reshape(2, peers, narrow, rows)
    turn_cos, turn_sin = angles(np.arange(peers), np.arange(rows), length)
    turn_cos = jnp.asarray(turn_cos[:, None, :], F32)
    turn_sin = jnp.asarray(turn_sin[:, None, :], F32)
    real = stage[0] * turn_cos + stage[1] * turn_sin
    imag = stage[1] * turn_cos - stage[0] * turn_sin
    which = (lax.axis_index("row") * narrow + jnp.arange(narrow, dtype=jnp.int32)) % GS
    sine = (which > GS // 2)[None, :, None]
    lead = jnp.where(sine, -imag, real)
    tail = jnp.where(sine, real, imag)
    turned = jnp.concatenate([lead, tail], axis=-1).astype(BF).reshape(channels, 2 * rows)
    long_cos, long_sin = angles(np.arange(rows), np.arange(rows), rows)
    second = jnp.asarray(np.concatenate([long_cos, long_sin], axis=1), BF)
    whole = dot(second, turned, ((1,), (1,))).astype(BF)

    back = lax.all_to_all(whole.reshape(peers, inner, channels), "row", split_axis=0, concat_axis=0, tiled=True)
    back = back.reshape(peers, inner, peers, narrow).transpose(1, 2, 0, 3).reshape(rows, channels)
    mixed_real = (dot(back, join_all) * (1.0 / math.sqrt(length * GS))).astype(BF)
    width = channels // len(out_parts)
    result = sum(
        dot(mixed_real[:, i * width : (i + 1) * width], part) for i, part in enumerate(out_parts)
    )
    return result.astype(BF)[None]


def swap(value, axis, count, bit):
    return lax.ppermute(value, axis, [(i, i ^ bit) for i in range(count)])


def row_index():
    return lax.axis_index("row").astype(jnp.int32)


def vmem_params():
    return pltpu.CompilerParams(vmem_limit_bytes=24 * 2**20)


def whole_specs(count):
    return [pl.BlockSpec(memory_space=pltpu.VMEM)] * count


def cost(flops, moved):
    return pl.CostEstimate(flops=int(flops), bytes_accessed=int(moved), transcendentals=0)


def norm_kernel(tokens_ref, gain_ref, out_ref):
    rows = tokens_ref[0].astype(F32)
    inverse_rms = lax.rsqrt(jnp.mean(rows * rows, axis=-1, keepdims=True) + EPS)
    out_ref[...] = (rows * inverse_rms * gain_ref[...].astype(F32)).astype(BF)


def norm_rows(tokens, gain):
    rows, width = tokens.shape[1:]
    step = rows // 6
    return pl.pallas_call(
        norm_kernel,
        out_shape=jax.ShapeDtypeStruct((rows, width), BF),
        grid=(rows // step,),
        in_specs=[
            pl.BlockSpec((1, step, width), lambda i: (0, i, 0)),
            pl.BlockSpec((1, width), lambda i: (0, 0)),
        ],
        out_specs=pl.BlockSpec((step, width), lambda i: (i, 0)),
        compiler_params=vmem_params(),
        cost_estimate=cost(rows * width * 2000, rows * width * 4),
        name="norm_rows",
    )(tokens, gain.reshape(1, width))


def features(normed_ref, me, near, depth, bits):
    at = me // near * near + lax.bitwise_xor(lax.rem(me, near), bits)
    across = lax.rem(at + near, 2 * near)
    return [normed_ref[:, pl.ds(pl.multiple_of(i * depth, depth), depth)] for i in (at, across)]


def project_most(normed, own, other, near):
    bits = list(own)
    depth, columns = own[0].shape[1:]
    rows = normed.shape[0]

    def kernel(normed_ref, *refs):
        out_ref = refs[-1]
        piece = jnp.concatenate([f for m in bits for f in features(normed_ref, row_index(), near, depth, m)], axis=1)
        for half in range(2):
            weight = [r[...].reshape(2 * depth, columns) for r in refs[half * len(bits) : (half + 1) * len(bits)]]
            product = jnp.dot(piece, jnp.concatenate(weight), preferred_element_type=F32)
            out_ref[:, half * columns : (half + 1) * columns] = product

    arrays = [own[m] for m in bits] + [other[m] for m in bits]
    return pl.pallas_call(
        kernel,
        out_shape=jax.ShapeDtypeStruct((rows, 2 * columns), F32),
        in_specs=whole_specs(1 + len(arrays)),
        out_specs=pl.BlockSpec(memory_space=pltpu.VMEM),
        compiler_params=vmem_params(),
        cost_estimate=cost(8 * rows * len(bits) * depth * columns, rows * columns * 8),
        name="project_most",
    )(normed, *arrays)


def project_last(normed, own, other, split, sofar, near):
    bits = list(own)
    depth, columns = own[bits[0]].shape[1:]
    rows = normed.shape[0]

    def kernel(normed_ref, split_ref, sofar_ref, *refs):
        out_ref = refs[-1]
        piece = jnp.concatenate([f for m in bits for f in features(normed_ref, row_index(), near, depth, m)], axis=1)
        for half in range(2):
            weight = [r[...].reshape(2 * depth, columns) for r in refs[half * len(bits) : (half + 1) * len(bits)]]
            total = jnp.dot(piece, jnp.concatenate(weight), preferred_element_type=F32)
            total = (total + sofar_ref[:, half * columns : (half + 1) * columns]).astype(BF)
            sums = dot(split_ref[...], total, ((1,), (1,)))
            out_ref[half * columns : (half + 1) * columns] = sums.astype(BF)

    arrays = [own[m] for m in bits] + [other[m] for m in bits]
    return pl.pallas_call(
        kernel,
        out_shape=jax.ShapeDtypeStruct((2 * columns, rows), BF),
        in_specs=whole_specs(3 + len(arrays)),
        out_specs=pl.BlockSpec(memory_space=pltpu.VMEM),
        compiler_params=vmem_params(),
        cost_estimate=cost(8 * rows * len(bits) * depth * columns, rows * columns * 4),
        name="project_last",
    )(normed, split, sofar, *arrays)


def sixteen(lines):
    wave = [2.0 * math.pi * i / 16 for i in range(16)]
    total = [lines[r] + lines[r + 8] for r in range(8)]
    left = [lines[r] - lines[r + 8] for r in range(8)]
    inner = [total[r] + total[r + 4] for r in range(4)]
    outer = [total[r] - total[r + 4] for r in range(4)]
    real, imag = {}, {}
    even, odd = inner[0] + inner[2], inner[1] + inner[3]
    real[0], real[8] = even + odd, even - odd
    imag[0] = imag[8] = jnp.zeros_like(even)
    real[4], imag[4] = inner[0] - inner[2], inner[3] - inner[1]
    root = math.sqrt(0.5)
    less, more = (outer[1] - outer[3]) * root, (outer[1] + outer[3]) * root
    real[2], real[6] = outer[0] + less, outer[0] - less
    imag[2], imag[6] = -more - outer[2], outer[2] - more
    cosine = [left[r] - left[8 - r] for r in range(1, 4)]
    sine = [left[r] + left[8 - r] for r in range(1, 4)]
    for k in (1, 3, 5, 7):
        real[k] = left[0] + sum(cosine[r - 1] * math.cos(wave[r * k % 16]) for r in range(1, 4))
        middle = left[4] * math.sin(wave[4 * k % 16])
        imag[k] = -middle - sum(sine[r - 1] * math.sin(wave[r * k % 16]) for r in range(1, 4))
    return real, imag


def transform_kernel(length, got_ref, second_ref, out_ref, lead_ref, tail_ref):
    channels, rows = got_ref.shape
    peers = length // rows
    narrow = channels // peers
    k = lax.broadcasted_iota(jnp.int32, (peers, rows), 0)
    m = lax.broadcasted_iota(jnp.int32, (peers, rows), 1)
    radians = lax.rem(k * m, length).astype(F32) * (2.0 * math.pi / length)
    cos, sin = jnp.cos(radians), jnp.sin(radians)
    high, wide = 16, 128
    for c in range(0, narrow, high):
        which = lax.broadcasted_iota(jnp.int32, (high, wide), 0) + row_index() * narrow + c
        sums = lax.rem(which, GS) > GS // 2
        for w in range(0, rows, wide):
            lines = [got_ref[r * narrow + c : r * narrow + c + high, w : w + wide].astype(F32) for r in range(peers)]
            real, imag = sixteen(lines)
            for f in range(peers):
                a, b = (real[f], imag[f]) if f <= peers // 2 else (real[peers - f], -imag[peers - f])
                tc, ts = cos[f : f + 1, w : w + wide], sin[f : f + 1, w : w + wide]
                first, other = a * tc + b * ts, b * tc - a * ts
                at = f * narrow + c
                lead_ref[at : at + high, w : w + wide] = jnp.where(sums, -other, first).astype(BF)
                tail_ref[at : at + high, w : w + wide] = jnp.where(sums, first, other).astype(BF)
    lanes = ((1,), (1,))
    out = dot(second_ref[:, :rows], lead_ref[...], lanes) + dot(second_ref[:, rows:], tail_ref[...], lanes)
    out_ref[...] = out.astype(BF)


def transform(got, peers, rows):
    channels = got.shape[0]
    long_cos, long_sin = angles(np.arange(rows), np.arange(rows), rows)
    second = jnp.asarray(np.concatenate([long_cos, long_sin], axis=1), BF)
    return pl.pallas_call(
        lambda *refs: transform_kernel(rows * peers, *refs),
        out_shape=jax.ShapeDtypeStruct((rows, channels), BF),
        in_specs=whole_specs(2),
        out_specs=pl.BlockSpec(memory_space=pltpu.VMEM),
        scratch_shapes=[pltpu.VMEM((channels, rows), BF), pltpu.VMEM((channels, rows), BF)],
        compiler_params=vmem_params(),
        cost_estimate=cost(4 * rows * channels * channels, 6 * channels * channels),
        name="transform",
    )(got, second)


def regroup(quads, lane):
    low, high = [], []
    for j in range(2):
        a, b = quads[j], quads[j + 2]
        low.append(jnp.where(lane < 64, a, pltpu.roll(b, 64, 1)))
        high.append(jnp.where(lane < 64, pltpu.roll(a, 64, 1), b))
    out = []
    even = lax.rem(lane, 64) < 32
    for e, o in (low, high):
        out.append(jnp.where(even, e, pltpu.roll(o, 32, 1)))
        out.append(jnp.where(even, pltpu.roll(e, 96, 1), o))
    return out


BLOCKS = {0: (0, 0), 4: (0, 2), 1: (1, 0), 5: (1, 2), 2: (2, 0), 6: (2, 2), 3: (3, 0), 7: (4, 0)}


def join_pattern(width):
    row = lax.broadcasted_iota(jnp.int32, (width, width), 0)
    column = lax.broadcasted_iota(jnp.int32, (width, width), 1)
    r, c = lax.rem(row, GS), lax.rem(column, GS)
    half = GS // 2
    cosine = r <= half
    order = jnp.where(cosine, r, r - half)
    straight = c == order
    turned = jnp.logical_and(c == GS - order, order < half)
    value = jnp.where(straight, jnp.where(cosine, 1.0, -1.0), jnp.where(turned, 1.0, 0.0))
    return jnp.where(row - r == column - c, value, 0.0).astype(BF)


def output_kernel(scale, depth, back_ref, *refs):
    own, other, (out_ref, sheet, made_ref, out_sem) = refs[:5], refs[5:10], refs[10:]
    peers, inner, channels = back_ref.shape
    near = len(BLOCKS)
    width = own[0].shape[2]
    lane = lax.broadcasted_iota(jnp.int32, (inner, 128), 1)
    quads = channels // 128
    for a in range(quads):
        for b in range(quads):
            tiles = [back_ref[4 * b + j, :, 128 * a : 128 * a + 128].astype(F32) for j in range(4)]
            for i, tile in enumerate(regroup(tiles, lane)):
                sheet[b, pl.ds(4 * a + i, inner, stride=peers), :] = tile
    join = join_pattern(128)
    joined = [jnp.dot(sheet[b].astype(BF), join, preferred_element_type=F32) * scale for b in range(quads)]
    mixed_real = jnp.concatenate([part.astype(BF) for part in joined], axis=1)
    upper = row_index() // near
    place = lax.rem(row_index(), near)
    stores = []
    for m, (source, start) in BLOCKS.items():
        left, right = [
            jnp.concatenate([arrays[source][start], arrays[source][start + 1]], axis=1) for arrays in (own, other)
        ]
        part = jnp.dot(mixed_real[:, :depth], left, preferred_element_type=F32)
        part = part + jnp.dot(mixed_real[:, depth:], right, preferred_element_type=F32)
        made_ref[m] = part.astype(BF)
        at = lax.bitwise_xor(place, m)
        for t, half in enumerate((upper, 1 - upper)):
            into = out_ref.at[:, pl.ds(pl.multiple_of((half * near + at) * width, width), width)]
            store = pltpu.make_async_copy(made_ref.at[m, :, t * width : t * width + width], into, out_sem.at[m, t])
            store.start()
            stores.append(store)
    for store in stores:
        store.wait()


def output(back, own, other, scale):
    peers, inner, channels = back.shape
    depth, width = own[0].shape[1:]
    rows = peers * inner
    near = len(BLOCKS)
    return pl.pallas_call(
        lambda *refs: output_kernel(scale, depth, *refs),
        out_shape=jax.ShapeDtypeStruct((rows, width * peers), BF),
        in_specs=whole_specs(1 + len(own) + len(other)),
        out_specs=pl.BlockSpec(memory_space=pltpu.HBM),
        scratch_shapes=[
            pltpu.VMEM((channels // 128, rows, 128), F32),
            pltpu.VMEM((near, rows, 2 * width), BF),
            pltpu.SemaphoreType.DMA((near, 2)),
        ],
        compiler_params=vmem_params(),
        cost_estimate=cost(2 * rows * channels * width * peers, rows * width * peers * 2),
        name="output",
    )(back, *own, *other)


ROUNDS = ((1, 0, 1), (2, 0, 2), (4, 0, 4), (5, 1, 4), (3, 2, 1), (6, 4, 2), (7, 5, 2))


LATE = (6, 7)


def body_cube(tokens, norm_gain, in_weight, out_weight):
    peers = lax.axis_size("row")
    cols = lax.axis_size("col")
    near = peers // 2
    rows = tokens.shape[1]
    channels = in_weight.shape[1] * cols
    narrow = channels // peers
    inner = rows // peers
    split, _ = group_tables()
    split_half = jnp.asarray(np.kron(np.eye(channels // cols // GS), split.T), BF)

    def row_swap(value, bit):
        return swap(value, "row", peers, bit)

    def core_swap(value):
        return swap(value, "col", cols, 1)

    in_far = row_swap(in_weight, near)
    normed = norm_rows(tokens, norm_gain)
    parts = {0: jnp.stack([in_weight, in_far])}
    for bits, source, bit in ROUNDS:
        parts[bits] = row_swap(parts[source], bit)
    mirror = {bits: core_swap(part) for bits, part in parts.items()}
    most = [bits for bits in parts if bits not in LATE]
    sofar = project_most(normed, {m: parts[m] for m in most}, {m: mirror[m] for m in most}, near)

    out_far = row_swap(out_weight, near)
    pair = jnp.stack([out_weight, out_far])
    beside = row_swap(pair, 4)
    quad = jnp.concatenate([pair, beside])
    over_x = row_swap(quad, 1)
    over_y = row_swap(quad, 2)
    over_xy = [row_swap(over_y[:2], 1), row_swap(over_x[2:], 2)]
    ours = [quad, over_x, over_y, *over_xy]
    others = [core_swap(value) for value in ours]

    sums = project_last(normed, {m: parts[m] for m in LATE}, {m: mirror[m] for m in LATE}, split_half, sofar, near)
    got = lax.all_to_all(sums.reshape(peers, narrow, rows), "row", split_axis=0, concat_axis=0, tiled=True)
    whole = transform(got.reshape(channels, rows), peers, rows)
    back = lax.all_to_all(whole.reshape(peers, inner, channels), "row", split_axis=0, concat_axis=0, tiled=True)
    scale = 1.0 / math.sqrt(rows * peers * GS)
    result = output(back, ours, others, scale)
    return result[None]


def body(tokens, norm_gain, in_weight, out_weight):
    peers, cols = lax.axis_size("row"), lax.axis_size("col")
    channels = in_weight.shape[1] * cols
    fits = tokens.shape[1] % (8 * peers) == 0 and in_weight.shape[0] % 128 == 0 and out_weight.shape[1] % 128 == 0
    if peers == 16 and cols == 2 and channels == 32 * peers and fits:
        return body_cube(tokens, norm_gain, in_weight, out_weight)
    return body_general(tokens, norm_gain, in_weight, out_weight)


def solution(mesh):
    in_specs = (P("col", "row", None), P(), P("row", "col"), P("col", "row"))
    out_specs = P("col", "row", None)
    return jax.shard_map(body, mesh=mesh, in_specs=in_specs, out_specs=out_specs, check_vma=False)
```

profile of v0, /device:TPU:0, one launch (start us, length us, event | category | flops | bytes accessed | tf_op | source)
XLA Modules:
  0.0 81.1 jit_solution(10837188544561338585)
XLA Ops:
  0.0 4.1 %collective-permute-start = (bf16[128,256]{1,0:T(8,128)(2,1)}, bf16[128,256]{1,0:T(8,128)(2,1)S(1)}, u32[]{:S(2)}, u32[]{:S(2)}) collective-permute-start(bf16[128,256]{1,0:T(8,128)(2,1)} %param.8), channel_id=1, source_target_pairs={{0,16},{2,18},{4,20},{6,22},{8,24},{10,26},{12,28},{14,30},{16,0},... | collective-permute-start | bytes 196616 | tf_op jit(solution)/shard_map/ppermute | solution.py:116
  4.1 3.9 %collective-permute-done = bf16[128,256]{1,0:T(8,128)(2,1)S(1)} collective-permute-done((bf16[128,256]{1,0:T(8,128)(2,1)}, bf16[128,256]{1,0:T(8,128)(2,1)S(1)}, u32[]{:S(2)}, u32[]{:S(2)}) %collective-permute-start) | collective-permute-done | bytes 65568 | tf_op jit(solution)/shard_map/ppermute | solution.py:116
  7.9 0.9 %pad_maximum_fusion.1.refs_0_ = bf16[2,128,256]{2,1,0:T(8,128)(2,1)S(1)} fusion(bf16[1,128,256]{2,1,0:T(8,128)(2,1)S(1)} %bitcast.14, bf16[1,128,256]{2,1,0:T(8,128)(2,1)} %bitcast.13), kind=kLoop, calls=%fused_computation.1 | loop fusion | flops 65536 | bytes 262144 | tf_op jit(solution)/shard_map/stack | solution.py:395
  8.8 1.8 %collective-permute-start.1 = (bf16[2,128,256]{2,1,0:T(8,128)(2,1)S(1)}, bf16[2,128,256]{2,1,0:T(8,128)(2,1)S(1)}, u32[]{:S(2)}, u32[]{:S(2)}) collective-permute-start(bf16[2,128,256]{2,1,0:T(8,128)(2,1)S(1)} %pad_maximum_fusion.1.refs_0_), channel_id=1, source_target_pairs={{0,2},{2,0},{4,6},{6,4},{8,10},{10,8},{12,14},{14,12},{16,18},{18,... | collective-permute-start | bytes 393224 | tf_op jit(solution)/shard_map/ppermute | solution.py:116
  10.5 1.5 %collective-permute-start.2 = (bf16[2,128,256]{2,1,0:T(8,128)(2,1)S(1)}, bf16[2,128,256]{2,1,0:T(8,128)(2,1)S(1)}, u32[]{:S(2)}, u32[]{:S(2)}) collective-permute-start(bf16[2,128,256]{2,1,0:T(8,128)(2,1)S(1)} %pad_maximum_fusion.1.refs_0_), channel_id=1, source_target_pairs={{0,4},{2,6},{4,0},{6,2},{8,12},{10,14},{12,8},{14,10},{16,20},{18,... | collective-permute-start | bytes 393224 | tf_op jit(solution)/shard_map/ppermute | solution.py:116
  12.5 1.3 %collective-permute-done.1.refs_1_ = bf16[2,128,256]{2,1,0:T(8,128)(2,1)S(1)} collective-permute-done((bf16[2,128,256]{2,1,0:T(8,128)(2,1)S(1)}, bf16[2,128,256]{2,1,0:T(8,128)(2,1)S(1)}, u32[]{:S(2)}, u32[]{:S(2)}) %collective-permute-start.1) | collective-permute-done | bytes 131104 | tf_op jit(solution)/shard_map/ppermute | solution.py:116
  13.8 0.7 collective-permute-start.4
  14.5 1.0 %collective-permute-done.2.refs_2_ = bf16[2,128,256]{2,1,0:T(8,128)(2,1)S(1)} collective-permute-done((bf16[2,128,256]{2,1,0:T(8,128)(2,1)S(1)}, bf16[2,128,256]{2,1,0:T(8,128)(2,1)S(1)}, u32[]{:S(2)}, u32[]{:S(2)}) %collective-permute-start.2) | collective-permute-done | bytes 131104 | tf_op jit(solution)/shard_map/ppermute | solution.py:116
  16.0 2.4 %collective-permute-done.3.refs_3_ = bf16[2,128,256]{2,1,0:T(8,128)(2,1)S(1)} collective-permute-done((bf16[2,128,256]{2,1,0:T(8,128)(2,1)S(1)}, bf16[2,128,256]{2,1,0:T(8,128)(2,1)S(1)}, u32[]{:S(2)}, u32[]{:S(2)}) %collective-permute-start.3) | collective-permute-done | bytes 131104 | tf_op jit(solution)/shard_map/ppermute | solution.py:116
  18.9 0.9 %collective-permute-done.4.refs_4_ = bf16[2,128,256]{2,1,0:T(8,128)(2,1)S(1)} collective-permute-done((bf16[2,128,256]{2,1,0:T(8,128)(2,1)S(1)}, bf16[2,128,256]{2,1,0:T(8,128)(2,1)S(1)}, u32[]{:S(2)}, u32[]{:S(2)}) %collective-permute-start.4) | collective-permute-done | bytes 131104 | tf_op jit(solution)/shard_map/ppermute | solution.py:116
  19.8 0.7 collective-permute-start.13
  20.5 0.7 reshape.12.gain_ref
  21.9 2.9 %collective-permute-done.12.refs_0_ = bf16[2,128,256]{2,1,0:T(8,128)(2,1)S(1)} collective-permute-done((bf16[2,128,256]{2,1,0:T(8,128)(2,1)S(1)}, bf16[2,128,256]{2,1,0:T(8,128)(2,1)S(1)}, u32[]{:S(2)}, u32[]{:S(2)}) %collective-permute-start.12) | collective-permute-done | bytes 131104 | tf_op jit(solution)/shard_map/ppermute | solution.py:116
  24.8 2.3 %collective-permute-done.13.refs_1_ = bf16[2,128,256]{2,1,0:T(8,128)(2,1)S(1)} collective-permute-done((bf16[2,128,256]{2,1,0:T(8,128)(2,1)S(1)}, bf16[2,128,256]{2,1,0:T(8,128)(2,1)S(1)}, u32[]{:S(2)}, u32[]{:S(2)}) %collective-permute-start.13) | collective-permute-done | bytes 131104 | tf_op jit(solution)/shard_map/ppermute | solution.py:116
  27.2 1.4 %copy-done.1 = bf16[1,384,2048]{2,1,0:T(8,128)(2,1)S(1)} copy-done((bf16[1,384,2048]{2,1,0:T(8,128)(2,1)S(1)}, bf16[1,384,2048]{2,1,0:T(8,128)(2,1)}, u32[]{:S(2)}) %copy-start.1) | copy-done | bytes 1572888
  28.6 1.0 %norm_rows.1.normed_ref = bf16[384,2048]{1,0:T(8,128)(2,1)S(1)} custom-call(bf16[1,384,2048]{2,1,0:T(8,128)(2,1)S(1)} %copy-done.1, bf16[1,2048]{1,0:T(2,128)(2,1)S(1)} %reshape.12.gain_ref), custom_call_target="tpu_custom_call" | custom-call | flops 1572864000 | bytes 3145728 | tf_op jit(solution)/shard_map/norm_rows/pallas_call | solution.py:144
  29.6 0.8 project_most.1.sofar_ref
  30.5 1.7 %project_last.1 = bf16[512,384]{1,0:T(8,128)(2,1)} custom-call(bf16[384,2048]{1,0:T(8,128)(2,1)S(1)} %norm_rows.1.normed_ref, bf16[256,256]{1,0:T(8,128)(2,1)S(1)} %copy-done, f32[384,512]{1,0:T(8,128)S(1)} %project_most.1.sofar_ref, bf16[2,128,256]{2,1,0:T(8,128)(2,1)S(1)} %collective-permute-done.12.refs_0_, ...), custom_call_target="tpu_custom_call" | custom-call | flops 201326592 | bytes 393216 | tf_op jit(solution)/shard_map/project_last/pallas_call | solution.py:206
  32.3 4.5 %all-to-all-start = ((bf16[16,32,384]{2,1,0:T(8,128)(2,1)}), bf16[16,32,384]{2,1,0:T(8,128)(2,1)S(1)}, u32[]{:S(2)}, u32[]{:S(2)}) async-start(bf16[16,32,384]{2,1,0:T(8,128)(2,1)} %bitcast.2), calls=%async_computation | async-start | bytes 786432 | tf_op jit(solution)/shard_map/all_to_all | solution.py:413
  36.8 2.9 %collective-permute-start.16 = (bf16[256,128]{1,0:T(8,128)(2,1)S(1)}, bf16[256,128]{1,0:T(8,128)(2,1)S(1)}, u32[]{:S(2)}, u32[]{:S(2)}) collective-permute-start(bf16[256,128]{1,0:T(8,128)(2,1)S(1)} %copy-done.3), channel_id=1, source_target_pairs={{0,16},{2,18},{4,20},{6,22},{8,24},{10,26},{12,28},{14,30},{16,0},... | collective-permute-start | bytes 196616 | tf_op jit(solution)/shard_map/ppermute | solution.py:116
  39.7 12.2 %collective-permute-done.16 = bf16[256,128]{1,0:T(8,128)(2,1)S(1)} collective-permute-done((bf16[256,128]{1,0:T(8,128)(2,1)S(1)}, bf16[256,128]{1,0:T(8,128)(2,1)S(1)}, u32[]{:S(2)}, u32[]{:S(2)}) %collective-permute-start.16) | collective-permute-done | bytes 65568 | tf_op jit(solution)/shard_map/ppermute | solution.py:116
  51.9 1.9 %transform.1 = bf16[384,512]{1,0:T(8,128)(2,1)} custom-call(bf16[512,384]{1,0:T(8,128)(2,1)S(1)} %bitcast.8, bf16[384,768]{1,0:T(8,128)(2,1)S(1)} %copy-done.2), custom_call_target="tpu_custom_call" | custom-call | flops 402653184 | bytes 1572864 | tf_op jit(solution)/shard_map/transform/pallas_call | solution.py:272
  53.8 5.2 %all-to-all-start.1 = ((bf16[16,24,512]{2,1,0:T(8,128)(2,1)}), bf16[16,24,512]{2,1,0:T(8,128)(2,1)S(1)}, u32[]{:S(2)}, u32[]{:S(2)}) async-start(bf16[16,24,512]{2,1,0:T(8,128)(2,1)} %bitcast.4), calls=%async_computation.1 | async-start | bytes 786432 | tf_op jit(solution)/shard_map/all_to_all | solution.py:415
  59.1 2.0 %collective-permute-start.19 = (bf16[4,256,128]{2,1,0:T(8,128)(2,1)S(1)}, bf16[4,256,128]{2,1,0:T(8,128)(2,1)S(1)}, u32[]{:S(2)}, u32[]{:S(2)}) collective-permute-start(bf16[4,256,128]{2,1,0:T(8,128)(2,1)S(1)} %pad_maximum_fusion.refs_1_), channel_id=1, source_target_pairs={{0,4},{2,6},{4,0},{6,2},{8,12},{10,14},{12,8},{14,10},{16,20},{18,... | collective-permute-start | bytes 786440 | tf_op jit(solution)/shard_map/ppermute | solution.py:116
  61.0 1.5 %collective-permute-start.18 = (bf16[4,256,128]{2,1,0:T(8,128)(2,1)S(1)}, bf16[4,256,128]{2,1,0:T(8,128)(2,1)S(1)}, u32[]{:S(2)}, u32[]{:S(2)}) collective-permute-start(bf16[4,256,128]{2,1,0:T(8,128)(2,1)S(1)} %pad_maximum_fusion.refs_1_), channel_id=1, source_target_pairs={{0,2},{2,0},{4,6},{6,4},{8,10},{10,8},{12,14},{14,12},{16,18},{18,... | collective-permute-start | bytes 786440 | tf_op jit(solution)/shard_map/ppermute | solution.py:116
  62.5 8.0 %collective-permute-done.19.refs_3_ = bf16[4,256,128]{2,1,0:T(8,128)(2,1)S(1)} collective-permute-done((bf16[4,256,128]{2,1,0:T(8,128)(2,1)S(1)}, bf16[4,256,128]{2,1,0:T(8,128)(2,1)S(1)}, u32[]{:S(2)}, u32[]{:S(2)}) %collective-permute-start.19) | collective-permute-done | bytes 262176 | tf_op jit(solution)/shard_map/ppermute | solution.py:116
  70.5 1.8 %collective-permute-start.20 = (bf16[2,256,128]{2,1,0:T(8,128)(2,1)S(1)}, bf16[2,256,128]{2,1,0:T(8,128)(2,1)S(1)}, u32[]{:S(2)}, u32[]{:S(2)}) collective-permute-start(bf16[2,256,128]{2,1,0:T(8,128)(2,1)S(1)} %slice.8), channel_id=1, source_target_pairs={{0,2},{2,0},{4,6},{6,4},{8,10},{10,8},{12,14},{14,12},{16,18},{18,... | collective-permute-start | bytes 393224 | tf_op jit(solution)/shard_map/ppermute | solution.py:116
  72.3 1.2 %collective-permute-start.21 = (bf16[2,256,128]{2,1,0:T(8,128)(2,1)S(1)}, bf16[2,256,128]{2,1,0:T(8,128)(2,1)S(1)}, u32[]{:S(2)}, u32[]{:S(2)}) collective-permute-start(bf16[2,256,128]{2,1,0:T(8,128)(2,1)S(1)} %slice.9), channel_id=1, source_target_pairs={{0,4},{2,6},{4,0},{6,2},{8,12},{10,14},{12,8},{14,10},{16,20},{18,... | collective-permute-start | bytes 393224 | tf_op jit(solution)/shard_map/ppermute | solution.py:116
  74.0 1.5 %collective-permute-done.20.refs_4_ = bf16[2,256,128]{2,1,0:T(8,128)(2,1)S(1)} collective-permute-done((bf16[2,256,128]{2,1,0:T(8,128)(2,1)S(1)}, bf16[2,256,128]{2,1,0:T(8,128)(2,1)S(1)}, u32[]{:S(2)}, u32[]{:S(2)}) %collective-permute-start.20) | collective-permute-done | bytes 131104 | tf_op jit(solution)/shard_map/ppermute | solution.py:116
  75.5 1.8 %collective-permute-done.21.refs_5_ = bf16[2,256,128]{2,1,0:T(8,128)(2,1)S(1)} collective-permute-done((bf16[2,256,128]{2,1,0:T(8,128)(2,1)S(1)}, bf16[2,256,128]{2,1,0:T(8,128)(2,1)S(1)}, u32[]{:S(2)}, u32[]{:S(2)}) %collective-permute-start.21) | collective-permute-done | bytes 131104 | tf_op jit(solution)/shard_map/ppermute | solution.py:116
  77.3 1.3 %collective-permute-done.26.refs_10_ = bf16[2,256,128]{2,1,0:T(8,128)(2,1)S(1)} collective-permute-done((bf16[2,256,128]{2,1,0:T(8,128)(2,1)S(1)}, bf16[2,256,128]{2,1,0:T(8,128)(2,1)S(1)}, u32[]{:S(2)}, u32[]{:S(2)}) %collective-permute-start.26) | collective-permute-done | bytes 131104 | tf_op jit(solution)/shard_map/ppermute | solution.py:116
  78.7 2.4 %output.1 = bf16[384,2048]{1,0:T(8,128)(2,1)} custom-call(bf16[16,24,512]{2,1,0:T(8,128)(2,1)S(1)} %all-to-all-done.1.refs_0_, bf16[4,256,128]{2,1,0:T(8,128)(2,1)S(1)} %pad_maximum_fusion.refs_1_, bf16[4,256,128]{2,1,0:T(8,128)(2,1)S(1)} %collective-permute-done.18.refs_2_, bf16[4,256,128]{2,1,0:T(8,128)(2,1)S(1)} %collective-permute-done.19.refs_3_, ...), custom_call_target="tpu_custom_call" | custom-call | flops 805306368 | bytes 1572864 | tf_op jit(solution)/shard_map/output/pallas_call | solution.py:354
  (45 shorter events, 2.8 us)
Async XLA Ops:
  0.0 7.9 %collective-permute-start = (bf16[128,256]{1,0:T(8,128)(2,1)}, bf16[128,256]{1,0:T(8,128)(2,1)S(1)}, u32[]{:S(2)}, u32[]{:S(2)}) collective-permute-start(bf16[128,256]{1,0:T(8,128)(2,1)} %param.8), channel_id=1, source_target_pairs={{0,16},{2,18},{4,20},{6,22},{8,24},{10,26},{12,28},{14,30},{16,0},... | collective-permute-start | bytes 196616 | tf_op jit(solution)/shard_map/ppermute | solution.py:116
  8.8 5.0 %collective-permute-start.1 = (bf16[2,128,256]{2,1,0:T(8,128)(2,1)S(1)}, bf16[2,128,256]{2,1,0:T(8,128)(2,1)S(1)}, u32[]{:S(2)}, u32[]{:S(2)}) collective-permute-start(bf16[2,128,256]{2,1,0:T(8,128)(2,1)S(1)} %pad_maximum_fusion.1.refs_0_), channel_id=1, source_target_pairs={{0,2},{2,0},{4,6},{6,4},{8,10},{10,8},{12,14},{14,12},{16,18},{18,... | collective-permute-start | bytes 393224 | tf_op jit(solution)/shard_map/ppermute | solution.py:116
  10.5 5.0 %collective-permute-start.2 = (bf16[2,128,256]{2,1,0:T(8,128)(2,1)S(1)}, bf16[2,128,256]{2,1,0:T(8,128)(2,1)S(1)}, u32[]{:S(2)}, u32[]{:S(2)}) collective-permute-start(bf16[2,128,256]{2,1,0:T(8,128)(2,1)S(1)} %pad_maximum_fusion.1.refs_0_), channel_id=1, source_target_pairs={{0,4},{2,6},{4,0},{6,2},{8,12},{10,14},{12,8},{14,10},{16,20},{18,... | collective-permute-start | bytes 393224 | tf_op jit(solution)/shard_map/ppermute | solution.py:116
  12.1 6.4 %collective-permute-start.3 = (bf16[2,128,256]{2,1,0:T(8,128)(2,1)S(1)}, bf16[2,128,256]{2,1,0:T(8,128)(2,1)S(1)}, u32[]{:S(2)}, u32[]{:S(2)}) collective-permute-start(bf16[2,128,256]{2,1,0:T(8,128)(2,1)S(1)} %pad_maximum_fusion.1.refs_0_), channel_id=1, source_target_pairs={{0,8},{2,10},{4,12},{6,14},{8,0},{10,2},{12,4},{14,6},{16,24},{18,... | collective-permute-start | bytes 393224 | tf_op jit(solution)/shard_map/ppermute | solution.py:116
  12.5 5.9 %collective-permute-start.6 = (bf16[2,128,256]{2,1,0:T(8,128)(2,1)S(1)}, bf16[2,128,256]{2,1,0:T(8,128)(2,1)S(1)}, u32[]{:S(2)}, u32[]{:S(2)}) collective-permute-start(bf16[2,128,256]{2,1,0:T(8,128)(2,1)S(1)} %pad_maximum_fusion.1.refs_0_), channel_id=1, source_target_pairs={{0,1},{1,0},{2,3},{3,2},{4,5},{5,4},{6,7},{7,6},{8,9},{9,8},{10,11... | collective-permute-start | bytes 393224 | tf_op jit(solution)/shard_map/ppermute | solution.py:116
  13.8 6.0 %collective-permute-start.4 = (bf16[2,128,256]{2,1,0:T(8,128)(2,1)S(1)}, bf16[2,128,256]{2,1,0:T(8,128)(2,1)S(1)}, u32[]{:S(2)}, u32[]{:S(2)}) collective-permute-start(bf16[2,128,256]{2,1,0:T(8,128)(2,1)S(1)} %collective-permute-done.1.refs_1_), channel_id=1, source_target_pairs={{0,8},{2,10},{4,12},{6,14},{8,0},{10,2},{12,4},{14,6},{16,24},{18,... | collective-permute-start | bytes 393224 | tf_op jit(solution)/shard_map/ppermute | solution.py:116
  15.5 5.7 %collective-permute-start.5 = (bf16[2,128,256]{2,1,0:T(8,128)(2,1)S(1)}, bf16[2,128,256]{2,1,0:T(8,128)(2,1)S(1)}, u32[]{:S(2)}, u32[]{:S(2)}) collective-permute-start(bf16[2,128,256]{2,1,0:T(8,128)(2,1)S(1)} %collective-permute-done.2.refs_2_), channel_id=1, source_target_pairs={{0,2},{2,0},{4,6},{6,4},{8,10},{10,8},{12,14},{14,12},{16,18},{18,... | collective-permute-start | bytes 393224 | tf_op jit(solution)/shard_map/ppermute | solution.py:116
  16.0 5.3 %collective-permute-start.7 = (bf16[2,128,256]{2,1,0:T(8,128)(2,1)S(1)}, bf16[2,128,256]{2,1,0:T(8,128)(2,1)S(1)}, u32[]{:S(2)}, u32[]{:S(2)}) collective-permute-start(bf16[2,128,256]{2,1,0:T(8,128)(2,1)S(1)} %collective-permute-done.1.refs_1_), channel_id=1, source_target_pairs={{0,1},{1,0},{2,3},{3,2},{4,5},{5,4},{6,7},{7,6},{8,9},{9,8},{10,11... | collective-permute-start | bytes 393224 | tf_op jit(solution)/shard_map/ppermute | solution.py:116
  18.4 3.4 %collective-permute-start.8 = (bf16[2,128,256]{2,1,0:T(8,128)(2,1)S(1)}, bf16[2,128,256]{2,1,0:T(8,128)(2,1)S(1)}, u32[]{:S(2)}, u32[]{:S(2)}) collective-permute-start(bf16[2,128,256]{2,1,0:T(8,128)(2,1)S(1)} %collective-permute-done.2.refs_2_), channel_id=1, source_target_pairs={{0,1},{1,0},{2,3},{3,2},{4,5},{5,4},{6,7},{7,6},{8,9},{9,8},{10,11... | collective-permute-start | bytes 393224 | tf_op jit(solution)/shard_map/ppermute | solution.py:116
  18.4 6.4 %collective-permute-start.12 = (bf16[2,128,256]{2,1,0:T(8,128)(2,1)S(1)}, bf16[2,128,256]{2,1,0:T(8,128)(2,1)S(1)}, u32[]{:S(2)}, u32[]{:S(2)}) collective-permute-start(bf16[2,128,256]{2,1,0:T(8,128)(2,1)S(1)} %collective-permute-done.3.refs_3_), channel_id=1, source_target_pairs={{0,4},{2,6},{4,0},{6,2},{8,12},{10,14},{12,8},{14,10},{16,20},{18,... | collective-permute-start | bytes 393224 | tf_op jit(solution)/shard_map/ppermute | solution.py:116
  19.8 7.3 %collective-permute-start.13 = (bf16[2,128,256]{2,1,0:T(8,128)(2,1)S(1)}, bf16[2,128,256]{2,1,0:T(8,128)(2,1)S(1)}, u32[]{:S(2)}, u32[]{:S(2)}) collective-permute-start(bf16[2,128,256]{2,1,0:T(8,128)(2,1)S(1)} %collective-permute-done.4.refs_4_), channel_id=1, source_target_pairs={{0,4},{2,6},{4,0},{6,2},{8,12},{10,14},{12,8},{14,10},{16,20},{18,... | collective-permute-start | bytes 393224 | tf_op jit(solution)/shard_map/ppermute | solution.py:116
  21.2 8.4 %collective-permute-start.9 = (bf16[2,128,256]{2,1,0:T(8,128)(2,1)S(1)}, bf16[2,128,256]{2,1,0:T(8,128)(2,1)S(1)}, u32[]{:S(2)}, u32[]{:S(2)}) collective-permute-start(bf16[2,128,256]{2,1,0:T(8,128)(2,1)S(1)} %collective-permute-done.3.refs_3_), channel_id=1, source_target_pairs={{0,1},{1,0},{2,3},{3,2},{4,5},{5,4},{6,7},{7,6},{8,9},{9,8},{10,11... | collective-permute-start | bytes 393224 | tf_op jit(solution)/shard_map/ppermute | solution.py:116
  21.3 8.3 %collective-permute-start.10 = (bf16[2,128,256]{2,1,0:T(8,128)(2,1)S(1)}, bf16[2,128,256]{2,1,0:T(8,128)(2,1)S(1)}, u32[]{:S(2)}, u32[]{:S(2)}) collective-permute-start(bf16[2,128,256]{2,1,0:T(8,128)(2,1)S(1)} %collective-permute-done.4.refs_4_), channel_id=1, source_target_pairs={{0,1},{1,0},{2,3},{3,2},{4,5},{5,4},{6,7},{7,6},{8,9},{9,8},{10,11... | collective-permute-start | bytes 393224 | tf_op jit(solution)/shard_map/ppermute | solution.py:116
  21.8 7.8 %collective-permute-start.11 = (bf16[2,128,256]{2,1,0:T(8,128)(2,1)S(1)}, bf16[2,128,256]{2,1,0:T(8,128)(2,1)S(1)}, u32[]{:S(2)}, u32[]{:S(2)}) collective-permute-start(bf16[2,128,256]{2,1,0:T(8,128)(2,1)S(1)} %collective-permute-done.5.refs_5_), channel_id=1, source_target_pairs={{0,1},{1,0},{2,3},{3,2},{4,5},{5,4},{6,7},{7,6},{8,9},{9,8},{10,11... | collective-permute-start | bytes 393224 | tf_op jit(solution)/shard_map/ppermute | solution.py:116
  24.8 5.7 %collective-permute-start.14 = (bf16[2,128,256]{2,1,0:T(8,128)(2,1)S(1)}, bf16[2,128,256]{2,1,0:T(8,128)(2,1)S(1)}, u32[]{:S(2)}, u32[]{:S(2)}) collective-permute-start(bf16[2,128,256]{2,1,0:T(8,128)(2,1)S(1)} %collective-permute-done.12.refs_0_), channel_id=1, source_target_pairs={{0,1},{1,0},{2,3},{3,2},{4,5},{5,4},{6,7},{7,6},{8,9},{9,8},{10,11... | collective-permute-start | bytes 393224 | tf_op jit(solution)/shard_map/ppermute | solution.py:116
  27.2 3.3 %collective-permute-start.15 = (bf16[2,128,256]{2,1,0:T(8,128)(2,1)S(1)}, bf16[2,128,256]{2,1,0:T(8,128)(2,1)S(1)}, u32[]{:S(2)}, u32[]{:S(2)}) collective-permute-start(bf16[2,128,256]{2,1,0:T(8,128)(2,1)S(1)} %collective-permute-done.13.refs_1_), channel_id=1, source_target_pairs={{0,1},{1,0},{2,3},{3,2},{4,5},{5,4},{6,7},{7,6},{8,9},{9,8},{10,11... | collective-permute-start | bytes 393224 | tf_op jit(solution)/shard_map/ppermute | solution.py:116
  27.2 1.4 %copy-start.1 = (bf16[1,384,2048]{2,1,0:T(8,128)(2,1)S(1)}, bf16[1,384,2048]{2,1,0:T(8,128)(2,1)}, u32[]{:S(2)}) copy-start(bf16[1,384,2048]{2,1,0:T(8,128)(2,1)} %tokens_ref.1) | copy-start | bytes 4718596
  30.5 6.3 %copy-start.3 = (bf16[256,128]{1,0:T(8,128)(2,1)S(1)}, bf16[256,128]{1,0:T(8,128)(2,1)}, u32[]{:S(2)}) copy-start(bf16[256,128]{1,0:T(8,128)(2,1)} %param.9) | copy-start | bytes 196612
  30.5 21.5 %copy-start.2 = (bf16[384,768]{1,0:T(8,128)(2,1)S(1)}, bf16[384,768]{1,0:T(8,128)(2,1)}, u32[]{:S(2)}) copy-start(bf16[384,768]{1,0:T(8,128)(2,1)} %constant.5.clone.refs_1_) | copy-start | bytes 1769476
  32.3 19.7 %all-to-all-start = ((bf16[16,32,384]{2,1,0:T(8,128)(2,1)}), bf16[16,32,384]{2,1,0:T(8,128)(2,1)S(1)}, u32[]{:S(2)}, u32[]{:S(2)}) async-start(bf16[16,32,384]{2,1,0:T(8,128)(2,1)} %bitcast.2), calls=%async_computation | async-start | bytes 786432 | tf_op jit(solution)/shard_map/all_to_all | solution.py:413
  36.8 15.1 %collective-permute-start.16 = (bf16[256,128]{1,0:T(8,128)(2,1)S(1)}, bf16[256,128]{1,0:T(8,128)(2,1)S(1)}, u32[]{:S(2)}, u32[]{:S(2)}) collective-permute-start(bf16[256,128]{1,0:T(8,128)(2,1)S(1)} %copy-done.3), channel_id=1, source_target_pairs={{0,16},{2,18},{4,20},{6,22},{8,24},{10,26},{12,28},{14,30},{16,0},... | collective-permute-start | bytes 196616 | tf_op jit(solution)/shard_map/ppermute | solution.py:116
  51.8 7.2 %collective-permute-start.17 = (bf16[2,256,128]{2,1,0:T(8,128)(2,1)S(1)}, bf16[2,256,128]{2,1,0:T(8,128)(2,1)S(1)}, u32[]{:S(2)}, u32[]{:S(2)}) collective-permute-start(bf16[2,256,128]{2,1,0:T(8,128)(2,1)S(1)} %pad_maximum_fusion.2), channel_id=1, source_target_pairs={{0,8},{2,10},{4,12},{6,14},{8,0},{10,2},{12,4},{14,6},{16,24},{18,... | collective-permute-start | bytes 393224 | tf_op jit(solution)/shard_map/ppermute | solution.py:116
  53.8 24.9 %all-to-all-start.1 = ((bf16[16,24,512]{2,1,0:T(8,128)(2,1)}), bf16[16,24,512]{2,1,0:T(8,128)(2,1)S(1)}, u32[]{:S(2)}, u32[]{:S(2)}) async-start(bf16[16,24,512]{2,1,0:T(8,128)(2,1)} %bitcast.4), calls=%async_computation.1 | async-start | bytes 786432 | tf_op jit(solution)/shard_map/all_to_all | solution.py:415
  59.1 11.4 %collective-permute-start.19 = (bf16[4,256,128]{2,1,0:T(8,128)(2,1)S(1)}, bf16[4,256,128]{2,1,0:T(8,128)(2,1)S(1)}, u32[]{:S(2)}, u32[]{:S(2)}) collective-permute-start(bf16[4,256,128]{2,1,0:T(8,128)(2,1)S(1)} %pad_maximum_fusion.refs_1_), channel_id=1, source_target_pairs={{0,4},{2,6},{4,0},{6,2},{8,12},{10,14},{12,8},{14,10},{16,20},{18,... | collective-permute-start | bytes 786440 | tf_op jit(solution)/shard_map/ppermute | solution.py:116
  61.0 11.2 %collective-permute-start.18 = (bf16[4,256,128]{2,1,0:T(8,128)(2,1)S(1)}, bf16[4,256,128]{2,1,0:T(8,128)(2,1)S(1)}, u32[]{:S(2)}, u32[]{:S(2)}) collective-permute-start(bf16[4,256,128]{2,1,0:T(8,128)(2,1)S(1)} %pad_maximum_fusion.refs_1_), channel_id=1, source_target_pairs={{0,2},{2,0},{4,6},{6,4},{8,10},{10,8},{12,14},{14,12},{16,18},{18,... | collective-permute-start | bytes 786440 | tf_op jit(solution)/shard_map/ppermute | solution.py:116
  62.5 14.8 %collective-permute-start.22 = (bf16[4,256,128]{2,1,0:T(8,128)(2,1)S(1)}, bf16[4,256,128]{2,1,0:T(8,128)(2,1)S(1)}, u32[]{:S(2)}, u32[]{:S(2)}) collective-permute-start(bf16[4,256,128]{2,1,0:T(8,128)(2,1)S(1)} %pad_maximum_fusion.refs_1_), channel_id=1, source_target_pairs={{0,1},{1,0},{2,3},{3,2},{4,5},{5,4},{6,7},{7,6},{8,9},{9,8},{10,11... | collective-permute-start | bytes 786440 | tf_op jit(solution)/shard_map/ppermute | solution.py:116
  70.5 5.0 %collective-permute-start.20 = (bf16[2,256,128]{2,1,0:T(8,128)(2,1)S(1)}, bf16[2,256,128]{2,1,0:T(8,128)(2,1)S(1)}, u32[]{:S(2)}, u32[]{:S(2)}) collective-permute-start(bf16[2,256,128]{2,1,0:T(8,128)(2,1)S(1)} %slice.8), channel_id=1, source_target_pairs={{0,2},{2,0},{4,6},{6,4},{8,10},{10,8},{12,14},{14,12},{16,18},{18,... | collective-permute-start | bytes 393224 | tf_op jit(solution)/shard_map/ppermute | solution.py:116
  72.3 5.0 %collective-permute-start.21 = (bf16[2,256,128]{2,1,0:T(8,128)(2,1)S(1)}, bf16[2,256,128]{2,1,0:T(8,128)(2,1)S(1)}, u32[]{:S(2)}, u32[]{:S(2)}) collective-permute-start(bf16[2,256,128]{2,1,0:T(8,128)(2,1)S(1)} %slice.9), channel_id=1, source_target_pairs={{0,4},{2,6},{4,0},{6,2},{8,12},{10,14},{12,8},{14,10},{16,20},{18,... | collective-permute-start | bytes 393224 | tf_op jit(solution)/shard_map/ppermute | solution.py:116
  73.5 5.2 %collective-permute-start.23 = (bf16[4,256,128]{2,1,0:T(8,128)(2,1)S(1)}, bf16[4,256,128]{2,1,0:T(8,128)(2,1)S(1)}, u32[]{:S(2)}, u32[]{:S(2)}) collective-permute-start(bf16[4,256,128]{2,1,0:T(8,128)(2,1)S(1)} %collective-permute-done.18.refs_2_), channel_id=1, source_target_pairs={{0,1},{1,0},{2,3},{3,2},{4,5},{5,4},{6,7},{7,6},{8,9},{9,8},{10,11... | collective-permute-start | bytes 786440 | tf_op jit(solution)/shard_map/ppermute | solution.py:116
  73.5 5.2 %collective-permute-start.24 = (bf16[4,256,128]{2,1,0:T(8,128)(2,1)S(1)}, bf16[4,256,128]{2,1,0:T(8,128)(2,1)S(1)}, u32[]{:S(2)}, u32[]{:S(2)}) collective-permute-start(bf16[4,256,128]{2,1,0:T(8,128)(2,1)S(1)} %collective-permute-done.19.refs_3_), channel_id=1, source_target_pairs={{0,1},{1,0},{2,3},{3,2},{4,5},{5,4},{6,7},{7,6},{8,9},{9,8},{10,11... | collective-permute-start | bytes 786440 | tf_op jit(solution)/shard_map/ppermute | solution.py:116
  75.5 1.8 %collective-permute-start.25 = (bf16[2,256,128]{2,1,0:T(8,128)(2,1)S(1)}, bf16[2,256,128]{2,1,0:T(8,128)(2,1)S(1)}, u32[]{:S(2)}, u32[]{:S(2)}) collective-permute-start(bf16[2,256,128]{2,1,0:T(8,128)(2,1)S(1)} %collective-permute-done.20.refs_4_), channel_id=1, source_target_pairs={{0,1},{1,0},{2,3},{3,2},{4,5},{5,4},{6,7},{7,6},{8,9},{9,8},{10,11... | collective-permute-start | bytes 393224 | tf_op jit(solution)/shard_map/ppermute | solution.py:116
  77.3 1.3 %collective-permute-start.26 = (bf16[2,256,128]{2,1,0:T(8,128)(2,1)S(1)}, bf16[2,256,128]{2,1,0:T(8,128)(2,1)S(1)}, u32[]{:S(2)}, u32[]{:S(2)}) collective-permute-start(bf16[2,256,128]{2,1,0:T(8,128)(2,1)S(1)} %collective-permute-done.21.refs_5_), channel_id=1, source_target_pairs={{0,1},{1,0},{2,3},{3,2},{4,5},{5,4},{6,7},{7,6},{8,9},{9,8},{10,11... | collective-permute-start | bytes 393224 | tf_op jit(solution)/shard_map/ppermute | solution.py:116
  (1 other events, 0.9 us)
where the time goes:
time: 81.5 us; the launch traced here: 81.1 us
  waiting for transfers between devices  39.6 us (49%)
  starting transfers between devices  30.4 us (37%)
  Pallas kernels  7.86 us (10%)
  local copies, waits for them, and re-layouts  2.15 us (3%)
  other arithmetic  0.9 us (1%)
    ppermute x27, waiting for transfers between devices, swap(): return lax.ppermute(value, axis, [(i, i ^ bit) for i in range(count)])  39.6 us
    ppermute x27, starting transfers between devices, swap(): return lax.ppermute(value, axis, [(i, i ^ bit) for i in range(count)])  20.7 us
    all_to_all x1, starting transfers between devices, body_cube(): lax.all_to_all(whole.reshape(peers, inner, channels), 'row', split_axis=0...  5.18 us
    all_to_all x1, starting transfers between devices, body_cube(): lax.all_to_all(sums.reshape(peers, narrow, rows), 'row', split_axis=0, co...  4.5 us
    pallas_call x1, Pallas kernels, output(): pl.pallas_call(lambda *refs: output_kernel(scale, depth, *refs), out_shap...  2.4 us
    pallas_call x1, Pallas kernels, transform(): pl.pallas_call(lambda *refs: transform_kernel(rows * peers, *refs), out_s...  1.89 us
    pallas_call x1, Pallas kernels, project_last(): pl.pallas_call(kernel, out_shape=jax.ShapeDtypeStruct((2 * columns, rows)...  1.75 us
  transfers between devices with their start and end apart: 29, of which 12 were waited for; matrix products, arithmetic and copies ran while one was open for 1% of the time, Pallas kernels for 5%

commit v1 on v0

--- a/solution.py
+++ b/solution.py
@@ -242,10 +242,8 @@
     channels, rows = got_ref.shape
     peers = length // rows
     narrow = channels // peers
-    k = lax.broadcasted_iota(jnp.int32, (peers, rows), 0)
-    m = lax.broadcasted_iota(jnp.int32, (peers, rows), 1)
-    radians = lax.rem(k * m, length).astype(F32) * (2.0 * math.pi / length)
-    cos, sin = jnp.cos(radians), jnp.sin(radians)
+    turns = second_ref[rows : rows + peers].astype(F32) + second_ref[rows + peers :].astype(F32)
+    cos, sin = turns[:, :rows], turns[:, rows:]
     high, wide = 16, 128
     for c in range(0, narrow, high):
         which = lax.broadcasted_iota(jnp.int32, (high, wide), 0) + row_index() * narrow + c
@@ -261,14 +259,17 @@
                 lead_ref[at : at + high, w : w + wide] = jnp.where(sums, -other, first).astype(BF)
                 tail_ref[at : at + high, w : w + wide] = jnp.where(sums, first, other).astype(BF)
     lanes = ((1,), (1,))
-    out = dot(second_ref[:, :rows], lead_ref[...], lanes) + dot(second_ref[:, rows:], tail_ref[...], lanes)
+    out = dot(second_ref[:rows, :rows], lead_ref[...], lanes) + dot(second_ref[:rows, rows:], tail_ref[...], lanes)
     out_ref[...] = out.astype(BF)
 
 
 def transform(got, peers, rows):
     channels = got.shape[0]
     long_cos, long_sin = angles(np.arange(rows), np.arange(rows), rows)
-    second = jnp.asarray(np.concatenate([long_cos, long_sin], axis=1), BF)
+    second = np.concatenate([long_cos, long_sin], axis=1)
+    turns = np.concatenate(angles(np.arange(peers), np.arange(rows), rows * peers), axis=1)
+    high = turns.astype(BF).astype(np.float64)
+    second = jnp.asarray(np.concatenate([second, high, turns - high]), BF)
     return pl.pallas_call(
         lambda *refs: transform_kernel(rows * peers, *refs),
         out_shape=jax.ShapeDtypeStruct((rows, channels), BF),
@@ -311,7 +312,7 @@
     return jnp.where(row - r == column - c, value, 0.0).astype(BF)
 
 
-def output_kernel(scale, depth, back_ref, *refs):
+def output_kernel(scale, back_ref, *refs):
     own, other, (out_ref, sheet, made_ref, out_sem) = refs[:5], refs[5:10], refs[10:]
     peers, inner, channels = back_ref.shape
     near = len(BLOCKS)
@@ -330,12 +331,10 @@
     place = lax.rem(row_index(), near)
     stores = []
     for m, (source, start) in BLOCKS.items():
-        left, right = [
-            jnp.concatenate([arrays[source][start], arrays[source][start + 1]], axis=1) for arrays in (own, other)
-        ]
-        part = jnp.dot(mixed_real[:, :depth], left, preferred_element_type=F32)
-        part = part + jnp.dot(mixed_real[:, depth:], right, preferred_element_type=F32)
-        made_ref[m] = part.astype(BF)
+        weight = jnp.concatenate(
+            [jnp.concatenate([a[source][start], a[source][start + 1]], axis=1) for a in (own, other)]
+        )
+        made_ref[m] = jnp.dot(mixed_real, weight, preferred_element_type=F32).astype(BF)
         at = lax.bitwise_xor(place, m)
         for t, half in enumerate((upper, 1 - upper)):
             into = out_ref.at[:, pl.ds(pl.multiple_of((half * near + at) * width, width), width)]
@@ -348,11 +347,11 @@
 
 def output(back, own, other, scale):
     peers, inner, channels = back.shape
-    depth, width = own[0].shape[1:]
+    _, width = own[0].shape[1:]
     rows = peers * inner
     near = len(BLOCKS)
     return pl.pallas_call(
-        lambda *refs: output_kernel(scale, depth, *refs),
+        lambda *refs: output_kernel(scale, *refs),
         out_shape=jax.ShapeDtypeStruct((rows, width * peers), BF),
         in_specs=whole_specs(1 + len(own) + len(other)),
         out_specs=pl.BlockSpec(memory_space=pltpu.HBM),
@@ -370,7 +369,7 @@
 ROUNDS = ((1, 0, 1), (2, 0, 2), (4, 0, 4), (5, 1, 4), (3, 2, 1), (6, 4, 2), (7, 5, 2))
 
 
-LATE = (6, 7)
+LATE = (7,)
 
 
 def body_cube(tokens, norm_gain, in_weight, out_weight):

time: 81.5 us -> 80 us (0.982)
  waiting for transfers between devices: 39.6 us -> 37.7 us
  starting transfers between devices: 30.4 us -> 31.3 us
    ppermute x27, waiting for transfers between devices: 39.6 us -> 37.7 us  [swap(): return lax.ppermute(value, axis, [(i, i ^ bit) for i in range(count)])]
    ppermute x27, starting transfers between devices: 20.7 us -> 21.7 us  [swap(): return lax.ppermute(value, axis, [(i, i ^ bit) for i in range(count)])]
where the time goes in v1:
time: 80 us; the launch traced here: 79.6 us
  waiting for transfers between devices  37.7 us (47%)
  starting transfers between devices  31.3 us (39%)
  Pallas kernels  7.44 us (9%)
  local copies, waits for them, and re-layouts  2.14 us (3%)
  other arithmetic  0.9 us (1%)
    ppermute x27, waiting for transfers between devices, swap(): return lax.ppermute(value, axis, [(i, i ^ bit) for i in range(count)])  37.7 us
    ppermute x27, starting transfers between devices, swap(): return lax.ppermute(value, axis, [(i, i ^ bit) for i in range(count)])  21.7 us
    all_to_all x1, starting transfers between devices, body_cube(): lax.all_to_all(whole.reshape(peers, inner, channels), 'row', split_axis=0...  5.18 us
    all_to_all x1, starting transfers between devices, body_cube(): lax.all_to_all(sums.reshape(peers, narrow, rows), 'row', split_axis=0, co...  4.41 us
    pallas_call x1, Pallas kernels, output(): pl.pallas_call(lambda *refs: output_kernel(scale, *refs), out_shape=jax.S...  2.3 us
    pallas_call x1, Pallas kernels, transform(): pl.pallas_call(lambda *refs: transform_kernel(rows * peers, *refs), out_s...  1.77 us
  transfers between devices with their start and end apart: 29, of which 12 were waited for; matrix products, arithmetic and copies ran while one was open for 1% of the time, Pallas kernels for 5%

profile of v1, /device:TPU:0, one launch (start us, length us, event | category | flops | bytes accessed | tf_op | source)
XLA Modules:
  0.0 79.6 jit_solution(10113653456661511063)
XLA Ops:
  0.0 4.1 %collective-permute-start = (bf16[128,256]{1,0:T(8,128)(2,1)}, bf16[128,256]{1,0:T(8,128)(2,1)S(1)}, u32[]{:S(2)}, u32[]{:S(2)}) collective-permute-start(bf16[128,256]{1,0:T(8,128)(2,1)} %param.8), channel_id=1, source_target_pairs={{0,16},{2,18},{4,20},{6,22},{8,24},{10,26},{12,28},{14,30},{16,0},... | collective-permute-start | bytes 196616 | tf_op jit(solution)/shard_map/ppermute | solution.py:116
  4.1 3.9 %collective-permute-done = bf16[128,256]{1,0:T(8,128)(2,1)S(1)} collective-permute-done((bf16[128,256]{1,0:T(8,128)(2,1)}, bf16[128,256]{1,0:T(8,128)(2,1)S(1)}, u32[]{:S(2)}, u32[]{:S(2)}) %collective-permute-start) | collective-permute-done | bytes 65568 | tf_op jit(solution)/shard_map/ppermute | solution.py:116
  7.9 0.9 %pad_maximum_fusion.1.refs_0_ = bf16[2,128,256]{2,1,0:T(8,128)(2,1)S(1)} fusion(bf16[1,128,256]{2,1,0:T(8,128)(2,1)S(1)} %bitcast.14, bf16[1,128,256]{2,1,0:T(8,128)(2,1)} %bitcast.13), kind=kLoop, calls=%fused_computation.1 | loop fusion | flops 65536 | bytes 262144 | tf_op jit(solution)/shard_map/stack | solution.py:394
  8.8 1.8 %collective-permute-start.1 = (bf16[2,128,256]{2,1,0:T(8,128)(2,1)S(1)}, bf16[2,128,256]{2,1,0:T(8,128)(2,1)S(1)}, u32[]{:S(2)}, u32[]{:S(2)}) collective-permute-start(bf16[2,128,256]{2,1,0:T(8,128)(2,1)S(1)} %pad_maximum_fusion.1.refs_0_), channel_id=1, source_target_pairs={{0,2},{2,0},{4,6},{6,4},{8,10},{10,8},{12,14},{14,12},{16,18},{18,... | collective-permute-start | bytes 393224 | tf_op jit(solution)/shard_map/ppermute | solution.py:116
  10.5 1.5 %collective-permute-start.2 = (bf16[2,128,256]{2,1,0:T(8,128)(2,1)S(1)}, bf16[2,128,256]{2,1,0:T(8,128)(2,1)S(1)}, u32[]{:S(2)}, u32[]{:S(2)}) collective-permute-start(bf16[2,128,256]{2,1,0:T(8,128)(2,1)S(1)} %pad_maximum_fusion.1.refs_0_), channel_id=1, source_target_pairs={{0,4},{2,6},{4,0},{6,2},{8,12},{10,14},{12,8},{14,10},{16,20},{18,... | collective-permute-start | bytes 393224 | tf_op jit(solution)/shard_map/ppermute | solution.py:116
  12.5 1.3 %collective-permute-done.1.refs_1_ = bf16[2,128,256]{2,1,0:T(8,128)(2,1)S(1)} collective-permute-done((bf16[2,128,256]{2,1,0:T(8,128)(2,1)S(1)}, bf16[2,128,256]{2,1,0:T(8,128)(2,1)S(1)}, u32[]{:S(2)}, u32[]{:S(2)}) %collective-permute-start.1) | collective-permute-done | bytes 131104 | tf_op jit(solution)/shard_map/ppermute | solution.py:116
  13.8 0.7 collective-permute-start.4
  14.5 1.0 %collective-permute-done.2.refs_2_ = bf16[2,128,256]{2,1,0:T(8,128)(2,1)S(1)} collective-permute-done((bf16[2,128,256]{2,1,0:T(8,128)(2,1)S(1)}, bf16[2,128,256]{2,1,0:T(8,128)(2,1)S(1)}, u32[]{:S(2)}, u32[]{:S(2)}) %collective-permute-start.2) | collective-permute-done | bytes 131104 | tf_op jit(solution)/shard_map/ppermute | solution.py:116
  16.0 2.4 %collective-permute-done.3.refs_3_ = bf16[2,128,256]{2,1,0:T(8,128)(2,1)S(1)} collective-permute-done((bf16[2,128,256]{2,1,0:T(8,128)(2,1)S(1)}, bf16[2,128,256]{2,1,0:T(8,128)(2,1)S(1)}, u32[]{:S(2)}, u32[]{:S(2)}) %collective-permute-start.3) | collective-permute-done | bytes 131104 | tf_op jit(solution)/shard_map/ppermute | solution.py:116
  18.9 0.5 collective-permute-start.8
  19.8 1.1 %collective-permute-start.14 = (bf16[2,128,256]{2,1,0:T(8,128)(2,1)S(1)}, bf16[2,128,256]{2,1,0:T(8,128)(2,1)S(1)}, u32[]{:S(2)}, u32[]{:S(2)}) collective-permute-start(bf16[2,128,256]{2,1,0:T(8,128)(2,1)S(1)} %collective-permute-done.4.refs_4_), channel_id=1, source_target_pairs={{0,4},{2,6},{4,0},{6,2},{8,12},{10,14},{12,8},{14,10},{16,20},{18,... | collective-permute-start | bytes 393224 | tf_op jit(solution)/shard_map/ppermute | solution.py:116
  21.0 0.7 reshape.12.gain_ref
  21.8 2.9 %collective-permute-done.6.refs_6_ = bf16[2,128,256]{2,1,0:T(8,128)(2,1)S(1)} collective-permute-done((bf16[2,128,256]{2,1,0:T(8,128)(2,1)S(1)}, bf16[2,128,256]{2,1,0:T(8,128)(2,1)S(1)}, u32[]{:S(2)}, u32[]{:S(2)}) %collective-permute-start.6) | collective-permute-done | bytes 131104 | tf_op jit(solution)/shard_map/ppermute | solution.py:116
  25.3 0.9 %collective-permute-done.14.refs_0_ = bf16[2,128,256]{2,1,0:T(8,128)(2,1)S(1)} collective-permute-done((bf16[2,128,256]{2,1,0:T(8,128)(2,1)S(1)}, bf16[2,128,256]{2,1,0:T(8,128)(2,1)S(1)}, u32[]{:S(2)}, u32[]{:S(2)}) %collective-permute-start.14) | collective-permute-done | bytes 131104 | tf_op jit(solution)/shard_map/ppermute | solution.py:116
  26.2 1.4 %copy-done.1 = bf16[1,384,2048]{2,1,0:T(8,128)(2,1)S(1)} copy-done((bf16[1,384,2048]{2,1,0:T(8,128)(2,1)S(1)}, bf16[1,384,2048]{2,1,0:T(8,128)(2,1)}, u32[]{:S(2)}) %copy-start.1) | copy-done | bytes 1572888
  27.6 1.0 %norm_rows.1.normed_ref = bf16[384,2048]{1,0:T(8,128)(2,1)S(1)} custom-call(bf16[1,384,2048]{2,1,0:T(8,128)(2,1)S(1)} %copy-done.1, bf16[1,2048]{1,0:T(2,128)(2,1)S(1)} %reshape.12.gain_ref), custom_call_target="tpu_custom_call" | custom-call | flops 1572864000 | bytes 3145728 | tf_op jit(solution)/shard_map/norm_rows/pallas_call | solution.py:144
  28.7 0.9 %project_most.1.sofar_ref = f32[384,512]{1,0:T(8,128)S(1)} custom-call(bf16[384,2048]{1,0:T(8,128)(2,1)S(1)} %norm_rows.1.normed_ref, bf16[2,128,256]{2,1,0:T(8,128)(2,1)S(1)} %pad_maximum_fusion.1.refs_0_, bf16[2,128,256]{2,1,0:T(8,128)(2,1)S(1)} %collective-permute-done.1.refs_1_, bf16[2,128,256]{2,1,0:T(8,128)(2,1)S(1)} %collective-permute-done.2.refs_2_, ...), custom_call_target="tpu_custom_call" | custom-call | flops 704643072 | bytes 786432 | tf_op jit(solution)/shard_map/project_most/pallas_call | solution.py:179
  29.7 1.4 %project_last.1 = bf16[512,384]{1,0:T(8,128)(2,1)} custom-call(bf16[384,2048]{1,0:T(8,128)(2,1)S(1)} %norm_rows.1.normed_ref, bf16[256,256]{1,0:T(8,128)(2,1)S(1)} %copy-done, f32[384,512]{1,0:T(8,128)S(1)} %project_most.1.sofar_ref, bf16[2,128,256]{2,1,0:T(8,128)(2,1)S(1)} %collective-permute-done.14.refs_0_, ...), custom_call_target="tpu_custom_call" | custom-call | flops 100663296 | bytes 393216 | tf_op jit(solution)/shard_map/project_last/pallas_call | solution.py:206
  31.1 4.4 %all-to-all-start = ((bf16[16,32,384]{2,1,0:T(8,128)(2,1)}), bf16[16,32,384]{2,1,0:T(8,128)(2,1)S(1)}, u32[]{:S(2)}, u32[]{:S(2)}) async-start(bf16[16,32,384]{2,1,0:T(8,128)(2,1)} %bitcast.2), calls=%async_computation | async-start | bytes 786432 | tf_op jit(solution)/shard_map/all_to_all | solution.py:412
  35.5 2.9 %collective-permute-start.16 = (bf16[256,128]{1,0:T(8,128)(2,1)S(1)}, bf16[256,128]{1,0:T(8,128)(2,1)S(1)}, u32[]{:S(2)}, u32[]{:S(2)}) collective-permute-start(bf16[256,128]{1,0:T(8,128)(2,1)S(1)} %copy-done.3), channel_id=1, source_target_pairs={{0,16},{2,18},{4,20},{6,22},{8,24},{10,26},{12,28},{14,30},{16,0},... | collective-permute-start | bytes 196616 | tf_op jit(solution)/shard_map/ppermute | solution.py:116
  38.4 12.2 %collective-permute-done.16 = bf16[256,128]{1,0:T(8,128)(2,1)S(1)} collective-permute-done((bf16[256,128]{1,0:T(8,128)(2,1)S(1)}, bf16[256,128]{1,0:T(8,128)(2,1)S(1)}, u32[]{:S(2)}, u32[]{:S(2)}) %collective-permute-start.16) | collective-permute-done | bytes 65568 | tf_op jit(solution)/shard_map/ppermute | solution.py:116
  50.7 1.8 %transform.1 = bf16[384,512]{1,0:T(8,128)(2,1)} custom-call(bf16[512,384]{1,0:T(8,128)(2,1)S(1)} %bitcast.8, bf16[416,768]{1,0:T(8,128)(2,1)S(1)} %copy-done.2), custom_call_target="tpu_custom_call" | custom-call | flops 402653184 | bytes 1572864 | tf_op jit(solution)/shard_map/transform/pallas_call | solution.py:273
  52.5 5.2 %all-to-all-start.1 = ((bf16[16,24,512]{2,1,0:T(8,128)(2,1)}), bf16[16,24,512]{2,1,0:T(8,128)(2,1)S(1)}, u32[]{:S(2)}, u32[]{:S(2)}) async-start(bf16[16,24,512]{2,1,0:T(8,128)(2,1)} %bitcast.4), calls=%async_computation.1 | async-start | bytes 786432 | tf_op jit(solution)/shard_map/all_to_all | solution.py:414
  57.7 2.0 %collective-permute-start.19 = (bf16[4,256,128]{2,1,0:T(8,128)(2,1)S(1)}, bf16[4,256,128]{2,1,0:T(8,128)(2,1)S(1)}, u32[]{:S(2)}, u32[]{:S(2)}) collective-permute-start(bf16[4,256,128]{2,1,0:T(8,128)(2,1)S(1)} %pad_maximum_fusion.refs_1_), channel_id=1, source_target_pairs={{0,4},{2,6},{4,0},{6,2},{8,12},{10,14},{12,8},{14,10},{16,20},{18,... | collective-permute-start | bytes 786440 | tf_op jit(solution)/shard_map/ppermute | solution.py:116
  59.7 1.5 %collective-permute-start.18 = (bf16[4,256,128]{2,1,0:T(8,128)(2,1)S(1)}, bf16[4,256,128]{2,1,0:T(8,128)(2,1)S(1)}, u32[]{:S(2)}, u32[]{:S(2)}) collective-permute-start(bf16[4,256,128]{2,1,0:T(8,128)(2,1)S(1)} %pad_maximum_fusion.refs_1_), channel_id=1, source_target_pairs={{0,2},{2,0},{4,6},{6,4},{8,10},{10,8},{12,14},{14,12},{16,18},{18,... | collective-permute-start | bytes 786440 | tf_op jit(solution)/shard_map/ppermute | solution.py:116
  61.2 8.0 %collective-permute-done.19.refs_3_ = bf16[4,256,128]{2,1,0:T(8,128)(2,1)S(1)} collective-permute-done((bf16[4,256,128]{2,1,0:T(8,128)(2,1)S(1)}, bf16[4,256,128]{2,1,0:T(8,128)(2,1)S(1)}, u32[]{:S(2)}, u32[]{:S(2)}) %collective-permute-start.19) | collective-permute-done | bytes 262176 | tf_op jit(solution)/shard_map/ppermute | solution.py:116
  69.1 1.8 %collective-permute-start.20 = (bf16[2,256,128]{2,1,0:T(8,128)(2,1)S(1)}, bf16[2,256,128]{2,1,0:T(8,128)(2,1)S(1)}, u32[]{:S(2)}, u32[]{:S(2)}) collective-permute-start(bf16[2,256,128]{2,1,0:T(8,128)(2,1)S(1)} %slice.8), channel_id=1, source_target_pairs={{0,2},{2,0},{4,6},{6,4},{8,10},{10,8},{12,14},{14,12},{16,18},{18,... | collective-permute-start | bytes 393224 | tf_op jit(solution)/shard_map/ppermute | solution.py:116
  70.9 1.2 %collective-permute-start.21 = (bf16[2,256,128]{2,1,0:T(8,128)(2,1)S(1)}, bf16[2,256,128]{2,1,0:T(8,128)(2,1)S(1)}, u32[]{:S(2)}, u32[]{:S(2)}) collective-permute-start(bf16[2,256,128]{2,1,0:T(8,128)(2,1)S(1)} %slice.9), channel_id=1, source_target_pairs={{0,4},{2,6},{4,0},{6,2},{8,12},{10,14},{12,8},{14,10},{16,20},{18,... | collective-permute-start | bytes 393224 | tf_op jit(solution)/shard_map/ppermute | solution.py:116
  72.6 1.5 %collective-permute-done.20.refs_4_ = bf16[2,256,128]{2,1,0:T(8,128)(2,1)S(1)} collective-permute-done((bf16[2,256,128]{2,1,0:T(8,128)(2,1)S(1)}, bf16[2,256,128]{2,1,0:T(8,128)(2,1)S(1)}, u32[]{:S(2)}, u32[]{:S(2)}) %collective-permute-start.20) | collective-permute-done | bytes 131104 | tf_op jit(solution)/shard_map/ppermute | solution.py:116
  74.2 1.8 %collective-permute-done.21.refs_5_ = bf16[2,256,128]{2,1,0:T(8,128)(2,1)S(1)} collective-permute-done((bf16[2,256,128]{2,1,0:T(8,128)(2,1)S(1)}, bf16[2,256,128]{2,1,0:T(8,128)(2,1)S(1)}, u32[]{:S(2)}, u32[]{:S(2)}) %collective-permute-start.21) | collective-permute-done | bytes 131104 | tf_op jit(solution)/shard_map/ppermute | solution.py:116
  76.0 1.3 %collective-permute-done.26.refs_10_ = bf16[2,256,128]{2,1,0:T(8,128)(2,1)S(1)} collective-permute-done((bf16[2,256,128]{2,1,0:T(8,128)(2,1)S(1)}, bf16[2,256,128]{2,1,0:T(8,128)(2,1)S(1)}, u32[]{:S(2)}, u32[]{:S(2)}) %collective-permute-start.26) | collective-permute-done | bytes 131104 | tf_op jit(solution)/shard_map/ppermute | solution.py:116
  77.3 2.3 %output.1 = bf16[384,2048]{1,0:T(8,128)(2,1)} custom-call(bf16[16,24,512]{2,1,0:T(8,128)(2,1)S(1)} %all-to-all-done.1.refs_0_, bf16[4,256,128]{2,1,0:T(8,128)(2,1)S(1)} %pad_maximum_fusion.refs_1_, bf16[4,256,128]{2,1,0:T(8,128)(2,1)S(1)} %collective-permute-done.18.refs_2_, bf16[4,256,128]{2,1,0:T(8,128)(2,1)S(1)} %collective-permute-done.19.refs_3_, ...), custom_call_target="tpu_custom_call" | custom-call | flops 805306368 | bytes 1572864 | tf_op jit(solution)/shard_map/output/pallas_call | solution.py:353
  (45 shorter events, 3.2 us)
Async XLA Ops:
  0.0 7.9 %collective-permute-start = (bf16[128,256]{1,0:T(8,128)(2,1)}, bf16[128,256]{1,0:T(8,128)(2,1)S(1)}, u32[]{:S(2)}, u32[]{:S(2)}) collective-permute-start(bf16[128,256]{1,0:T(8,128)(2,1)} %param.8), channel_id=1, source_target_pairs={{0,16},{2,18},{4,20},{6,22},{8,24},{10,26},{12,28},{14,30},{16,0},... | collective-permute-start | bytes 196616 | tf_op jit(solution)/shard_map/ppermute | solution.py:116
  8.8 5.0 %collective-permute-start.1 = (bf16[2,128,256]{2,1,0:T(8,128)(2,1)S(1)}, bf16[2,128,256]{2,1,0:T(8,128)(2,1)S(1)}, u32[]{:S(2)}, u32[]{:S(2)}) collective-permute-start(bf16[2,128,256]{2,1,0:T(8,128)(2,1)S(1)} %pad_maximum_fusion.1.refs_0_), channel_id=1, source_target_pairs={{0,2},{2,0},{4,6},{6,4},{8,10},{10,8},{12,14},{14,12},{16,18},{18,... | collective-permute-start | bytes 393224 | tf_op jit(solution)/shard_map/ppermute | solution.py:116
  10.5 5.0 %collective-permute-start.2 = (bf16[2,128,256]{2,1,0:T(8,128)(2,1)S(1)}, bf16[2,128,256]{2,1,0:T(8,128)(2,1)S(1)}, u32[]{:S(2)}, u32[]{:S(2)}) collective-permute-start(bf16[2,128,256]{2,1,0:T(8,128)(2,1)S(1)} %pad_maximum_fusion.1.refs_0_), channel_id=1, source_target_pairs={{0,4},{2,6},{4,0},{6,2},{8,12},{10,14},{12,8},{14,10},{16,20},{18,... | collective-permute-start | bytes 393224 | tf_op jit(solution)/shard_map/ppermute | solution.py:116
  12.1 6.4 %collective-permute-start.3 = (bf16[2,128,256]{2,1,0:T(8,128)(2,1)S(1)}, bf16[2,128,256]{2,1,0:T(8,128)(2,1)S(1)}, u32[]{:S(2)}, u32[]{:S(2)}) collective-permute-start(bf16[2,128,256]{2,1,0:T(8,128)(2,1)S(1)} %pad_maximum_fusion.1.refs_0_), channel_id=1, source_target_pairs={{0,8},{2,10},{4,12},{6,14},{8,0},{10,2},{12,4},{14,6},{16,24},{18,... | collective-permute-start | bytes 393224 | tf_op jit(solution)/shard_map/ppermute | solution.py:116
  12.5 6.4 %collective-permute-start.7 = (bf16[2,128,256]{2,1,0:T(8,128)(2,1)S(1)}, bf16[2,128,256]{2,1,0:T(8,128)(2,1)S(1)}, u32[]{:S(2)}, u32[]{:S(2)}) collective-permute-start(bf16[2,128,256]{2,1,0:T(8,128)(2,1)S(1)} %pad_maximum_fusion.1.refs_0_), channel_id=1, source_target_pairs={{0,1},{1,0},{2,3},{3,2},{4,5},{5,4},{6,7},{7,6},{8,9},{9,8},{10,11... | collective-permute-start | bytes 393224 | tf_op jit(solution)/shard_map/ppermute | solution.py:116
  13.8 6.0 %collective-permute-start.4 = (bf16[2,128,256]{2,1,0:T(8,128)(2,1)S(1)}, bf16[2,128,256]{2,1,0:T(8,128)(2,1)S(1)}, u32[]{:S(2)}, u32[]{:S(2)}) collective-permute-start(bf16[2,128,256]{2,1,0:T(8,128)(2,1)S(1)} %collective-permute-done.1.refs_1_), channel_id=1, source_target_pairs={{0,8},{2,10},{4,12},{6,14},{8,0},{10,2},{12,4},{14,6},{16,24},{18,... | collective-permute-start | bytes 393224 | tf_op jit(solution)/shard_map/ppermute | solution.py:116
  15.5 6.2 %collective-permute-start.5 = (bf16[2,128,256]{2,1,0:T(8,128)(2,1)S(1)}, bf16[2,128,256]{2,1,0:T(8,128)(2,1)S(1)}, u32[]{:S(2)}, u32[]{:S(2)}) collective-permute-start(bf16[2,128,256]{2,1,0:T(8,128)(2,1)S(1)} %collective-permute-done.2.refs_2_), channel_id=1, source_target_pairs={{0,2},{2,0},{4,6},{6,4},{8,10},{10,8},{12,14},{14,12},{16,18},{18,... | collective-permute-start | bytes 393224 | tf_op jit(solution)/shard_map/ppermute | solution.py:116
  18.4 6.2 %collective-permute-start.6 = (bf16[2,128,256]{2,1,0:T(8,128)(2,1)S(1)}, bf16[2,128,256]{2,1,0:T(8,128)(2,1)S(1)}, u32[]{:S(2)}, u32[]{:S(2)}) collective-permute-start(bf16[2,128,256]{2,1,0:T(8,128)(2,1)S(1)} %collective-permute-done.3.refs_3_), channel_id=1, source_target_pairs={{0,4},{2,6},{4,0},{6,2},{8,12},{10,14},{12,8},{14,10},{16,20},{18,... | collective-permute-start | bytes 393224 | tf_op jit(solution)/shard_map/ppermute | solution.py:116
  18.9 5.7 %collective-permute-start.10 = (bf16[2,128,256]{2,1,0:T(8,128)(2,1)S(1)}, bf16[2,128,256]{2,1,0:T(8,128)(2,1)S(1)}, u32[]{:S(2)}, u32[]{:S(2)}) collective-permute-start(bf16[2,128,256]{2,1,0:T(8,128)(2,1)S(1)} %collective-permute-done.3.refs_3_), channel_id=1, source_target_pairs={{0,1},{1,0},{2,3},{3,2},{4,5},{5,4},{6,7},{7,6},{8,9},{9,8},{10,11... | collective-permute-start | bytes 393224 | tf_op jit(solution)/shard_map/ppermute | solution.py:116
  18.9 6.3 %collective-permute-start.8 = (bf16[2,128,256]{2,1,0:T(8,128)(2,1)S(1)}, bf16[2,128,256]{2,1,0:T(8,128)(2,1)S(1)}, u32[]{:S(2)}, u32[]{:S(2)}) collective-permute-start(bf16[2,128,256]{2,1,0:T(8,128)(2,1)S(1)} %collective-permute-done.1.refs_1_), channel_id=1, source_target_pairs={{0,1},{1,0},{2,3},{3,2},{4,5},{5,4},{6,7},{7,6},{8,9},{9,8},{10,11... | collective-permute-start | bytes 393224 | tf_op jit(solution)/shard_map/ppermute | solution.py:116
  19.8 6.4 %collective-permute-start.14 = (bf16[2,128,256]{2,1,0:T(8,128)(2,1)S(1)}, bf16[2,128,256]{2,1,0:T(8,128)(2,1)S(1)}, u32[]{:S(2)}, u32[]{:S(2)}) collective-permute-start(bf16[2,128,256]{2,1,0:T(8,128)(2,1)S(1)} %collective-permute-done.4.refs_4_), channel_id=1, source_target_pairs={{0,4},{2,6},{4,0},{6,2},{8,12},{10,14},{12,8},{14,10},{16,20},{18,... | collective-permute-start | bytes 393224 | tf_op jit(solution)/shard_map/ppermute | solution.py:116
  21.7 7.0 %collective-permute-start.9 = (bf16[2,128,256]{2,1,0:T(8,128)(2,1)S(1)}, bf16[2,128,256]{2,1,0:T(8,128)(2,1)S(1)}, u32[]{:S(2)}, u32[]{:S(2)}) collective-permute-start(bf16[2,128,256]{2,1,0:T(8,128)(2,1)S(1)} %collective-permute-done.2.refs_2_), channel_id=1, source_target_pairs={{0,1},{1,0},{2,3},{3,2},{4,5},{5,4},{6,7},{7,6},{8,9},{9,8},{10,11... | collective-permute-start | bytes 393224 | tf_op jit(solution)/shard_map/ppermute | solution.py:116
  24.7 4.0 %collective-permute-start.11 = (bf16[2,128,256]{2,1,0:T(8,128)(2,1)S(1)}, bf16[2,128,256]{2,1,0:T(8,128)(2,1)S(1)}, u32[]{:S(2)}, u32[]{:S(2)}) collective-permute-start(bf16[2,128,256]{2,1,0:T(8,128)(2,1)S(1)} %collective-permute-done.4.refs_4_), channel_id=1, source_target_pairs={{0,1},{1,0},{2,3},{3,2},{4,5},{5,4},{6,7},{7,6},{8,9},{9,8},{10,11... | collective-permute-start | bytes 393224 | tf_op jit(solution)/shard_map/ppermute | solution.py:116
  24.7 4.0 %collective-permute-start.12 = (bf16[2,128,256]{2,1,0:T(8,128)(2,1)S(1)}, bf16[2,128,256]{2,1,0:T(8,128)(2,1)S(1)}, u32[]{:S(2)}, u32[]{:S(2)}) collective-permute-start(bf16[2,128,256]{2,1,0:T(8,128)(2,1)S(1)} %collective-permute-done.5.refs_5_), channel_id=1, source_target_pairs={{0,1},{1,0},{2,3},{3,2},{4,5},{5,4},{6,7},{7,6},{8,9},{9,8},{10,11... | collective-permute-start | bytes 393224 | tf_op jit(solution)/shard_map/ppermute | solution.py:116
  25.2 3.5 %collective-permute-start.13 = (bf16[2,128,256]{2,1,0:T(8,128)(2,1)S(1)}, bf16[2,128,256]{2,1,0:T(8,128)(2,1)S(1)}, u32[]{:S(2)}, u32[]{:S(2)}) collective-permute-start(bf16[2,128,256]{2,1,0:T(8,128)(2,1)S(1)} %collective-permute-done.6.refs_6_), channel_id=1, source_target_pairs={{0,1},{1,0},{2,3},{3,2},{4,5},{5,4},{6,7},{7,6},{8,9},{9,8},{10,11... | collective-permute-start | bytes 393224 | tf_op jit(solution)/shard_map/ppermute | solution.py:116
  26.2 3.4 %collective-permute-start.15 = (bf16[2,128,256]{2,1,0:T(8,128)(2,1)S(1)}, bf16[2,128,256]{2,1,0:T(8,128)(2,1)S(1)}, u32[]{:S(2)}, u32[]{:S(2)}) collective-permute-start(bf16[2,128,256]{2,1,0:T(8,128)(2,1)S(1)} %collective-permute-done.14.refs_0_), channel_id=1, source_target_pairs={{0,1},{1,0},{2,3},{3,2},{4,5},{5,4},{6,7},{7,6},{8,9},{9,8},{10,11... | collective-permute-start | bytes 393224 | tf_op jit(solution)/shard_map/ppermute | solution.py:116
  26.2 1.4 %copy-start.1 = (bf16[1,384,2048]{2,1,0:T(8,128)(2,1)S(1)}, bf16[1,384,2048]{2,1,0:T(8,128)(2,1)}, u32[]{:S(2)}) copy-start(bf16[1,384,2048]{2,1,0:T(8,128)(2,1)} %tokens_ref.1) | copy-start | bytes 4718596
  29.6 5.9 %copy-start.3 = (bf16[256,128]{1,0:T(8,128)(2,1)S(1)}, bf16[256,128]{1,0:T(8,128)(2,1)}, u32[]{:S(2)}) copy-start(bf16[256,128]{1,0:T(8,128)(2,1)} %param.9) | copy-start | bytes 196612
  29.6 21.1 %copy-start.2 = (bf16[416,768]{1,0:T(8,128)(2,1)S(1)}, bf16[416,768]{1,0:T(8,128)(2,1)}, u32[]{:S(2)}) copy-start(bf16[416,768]{1,0:T(8,128)(2,1)} %constant.5.clone.refs_1_) | copy-start | bytes 1916932
  31.1 19.6 %all-to-all-start = ((bf16[16,32,384]{2,1,0:T(8,128)(2,1)}), bf16[16,32,384]{2,1,0:T(8,128)(2,1)S(1)}, u32[]{:S(2)}, u32[]{:S(2)}) async-start(bf16[16,32,384]{2,1,0:T(8,128)(2,1)} %bitcast.2), calls=%async_computation | async-start | bytes 786432 | tf_op jit(solution)/shard_map/all_to_all | solution.py:412
  35.5 15.0 %collective-permute-start.16 = (bf16[256,128]{1,0:T(8,128)(2,1)S(1)}, bf16[256,128]{1,0:T(8,128)(2,1)S(1)}, u32[]{:S(2)}, u32[]{:S(2)}) collective-permute-start(bf16[256,128]{1,0:T(8,128)(2,1)S(1)} %copy-done.3), channel_id=1, source_target_pairs={{0,16},{2,18},{4,20},{6,22},{8,24},{10,26},{12,28},{14,30},{16,0},... | collective-permute-start | bytes 196616 | tf_op jit(solution)/shard_map/ppermute | solution.py:116
  50.6 7.1 %collective-permute-start.17 = (bf16[2,256,128]{2,1,0:T(8,128)(2,1)S(1)}, bf16[2,256,128]{2,1,0:T(8,128)(2,1)S(1)}, u32[]{:S(2)}, u32[]{:S(2)}) collective-permute-start(bf16[2,256,128]{2,1,0:T(8,128)(2,1)S(1)} %pad_maximum_fusion.2), channel_id=1, source_target_pairs={{0,8},{2,10},{4,12},{6,14},{8,0},{10,2},{12,4},{14,6},{16,24},{18,... | collective-permute-start | bytes 393224 | tf_op jit(solution)/shard_map/ppermute | solution.py:116
  52.5 24.9 %all-to-all-start.1 = ((bf16[16,24,512]{2,1,0:T(8,128)(2,1)}), bf16[16,24,512]{2,1,0:T(8,128)(2,1)S(1)}, u32[]{:S(2)}, u32[]{:S(2)}) async-start(bf16[16,24,512]{2,1,0:T(8,128)(2,1)} %bitcast.4), calls=%async_computation.1 | async-start | bytes 786432 | tf_op jit(solution)/shard_map/all_to_all | solution.py:414
  57.7 11.4 %collective-permute-start.19 = (bf16[4,256,128]{2,1,0:T(8,128)(2,1)S(1)}, bf16[4,256,128]{2,1,0:T(8,128)(2,1)S(1)}, u32[]{:S(2)}, u32[]{:S(2)}) collective-permute-start(bf16[4,256,128]{2,1,0:T(8,128)(2,1)S(1)} %pad_maximum_fusion.refs_1_), channel_id=1, source_target_pairs={{0,4},{2,6},{4,0},{6,2},{8,12},{10,14},{12,8},{14,10},{16,20},{18,... | collective-permute-start | bytes 786440 | tf_op jit(solution)/shard_map/ppermute | solution.py:116
  59.7 11.2 %collective-permute-start.18 = (bf16[4,256,128]{2,1,0:T(8,128)(2,1)S(1)}, bf16[4,256,128]{2,1,0:T(8,128)(2,1)S(1)}, u32[]{:S(2)}, u32[]{:S(2)}) collective-permute-start(bf16[4,256,128]{2,1,0:T(8,128)(2,1)S(1)} %pad_maximum_fusion.refs_1_), channel_id=1, source_target_pairs={{0,2},{2,0},{4,6},{6,4},{8,10},{10,8},{12,14},{14,12},{16,18},{18,... | collective-permute-start | bytes 786440 | tf_op jit(solution)/shard_map/ppermute | solution.py:116
  61.1 14.8 %collective-permute-start.22 = (bf16[4,256,128]{2,1,0:T(8,128)(2,1)S(1)}, bf16[4,256,128]{2,1,0:T(8,128)(2,1)S(1)}, u32[]{:S(2)}, u32[]{:S(2)}) collective-permute-start(bf16[4,256,128]{2,1,0:T(8,128)(2,1)S(1)} %pad_maximum_fusion.refs_1_), channel_id=1, source_target_pairs={{0,1},{1,0},{2,3},{3,2},{4,5},{5,4},{6,7},{7,6},{8,9},{9,8},{10,11... | collective-permute-start | bytes 786440 | tf_op jit(solution)/shard_map/ppermute | solution.py:116
  69.1 5.0 %collective-permute-start.20 = (bf16[2,256,128]{2,1,0:T(8,128)(2,1)S(1)}, bf16[2,256,128]{2,1,0:T(8,128)(2,1)S(1)}, u32[]{:S(2)}, u32[]{:S(2)}) collective-permute-start(bf16[2,256,128]{2,1,0:T(8,128)(2,1)S(1)} %slice.8), channel_id=1, source_target_pairs={{0,2},{2,0},{4,6},{6,4},{8,10},{10,8},{12,14},{14,12},{16,18},{18,... | collective-permute-start | bytes 393224 | tf_op jit(solution)/shard_map/ppermute | solution.py:116
  70.9 5.0 %collective-permute-start.21 = (bf16[2,256,128]{2,1,0:T(8,128)(2,1)S(1)}, bf16[2,256,128]{2,1,0:T(8,128)(2,1)S(1)}, u32[]{:S(2)}, u32[]{:S(2)}) collective-permute-start(bf16[2,256,128]{2,1,0:T(8,128)(2,1)S(1)} %slice.9), channel_id=1, source_target_pairs={{0,4},{2,6},{4,0},{6,2},{8,12},{10,14},{12,8},{14,10},{16,20},{18,... | collective-permute-start | bytes 393224 | tf_op jit(solution)/shard_map/ppermute | solution.py:116
  72.1 5.2 %collective-permute-start.23 = (bf16[4,256,128]{2,1,0:T(8,128)(2,1)S(1)}, bf16[4,256,128]{2,1,0:T(8,128)(2,1)S(1)}, u32[]{:S(2)}, u32[]{:S(2)}) collective-permute-start(bf16[4,256,128]{2,1,0:T(8,128)(2,1)S(1)} %collective-permute-done.18.refs_2_), channel_id=1, source_target_pairs={{0,1},{1,0},{2,3},{3,2},{4,5},{5,4},{6,7},{7,6},{8,9},{9,8},{10,11... | collective-permute-start | bytes 786440 | tf_op jit(solution)/shard_map/ppermute | solution.py:116
  72.1 5.2 %collective-permute-start.24 = (bf16[4,256,128]{2,1,0:T(8,128)(2,1)S(1)}, bf16[4,256,128]{2,1,0:T(8,128)(2,1)S(1)}, u32[]{:S(2)}, u32[]{:S(2)}) collective-permute-start(bf16[4,256,128]{2,1,0:T(8,128)(2,1)S(1)} %collective-permute-done.19.refs_3_), channel_id=1, source_target_pairs={{0,1},{1,0},{2,3},{3,2},{4,5},{5,4},{6,7},{7,6},{8,9},{9,8},{10,11... | collective-permute-start | bytes 786440 | tf_op jit(solution)/shard_map/ppermute | solution.py:116
  74.2 1.8 %collective-permute-start.25 = (bf16[2,256,128]{2,1,0:T(8,128)(2,1)S(1)}, bf16[2,256,128]{2,1,0:T(8,128)(2,1)S(1)}, u32[]{:S(2)}, u32[]{:S(2)}) collective-permute-start(bf16[2,256,128]{2,1,0:T(8,128)(2,1)S(1)} %collective-permute-done.20.refs_4_), channel_id=1, source_target_pairs={{0,1},{1,0},{2,3},{3,2},{4,5},{5,4},{6,7},{7,6},{8,9},{9,8},{10,11... | collective-permute-start | bytes 393224 | tf_op jit(solution)/shard_map/ppermute | solution.py:116
  76.0 1.3 %collective-permute-start.26 = (bf16[2,256,128]{2,1,0:T(8,128)(2,1)S(1)}, bf16[2,256,128]{2,1,0:T(8,128)(2,1)S(1)}, u32[]{:S(2)}, u32[]{:S(2)}) collective-permute-start(bf16[2,256,128]{2,1,0:T(8,128)(2,1)S(1)} %collective-permute-done.21.refs_5_), channel_id=1, source_target_pairs={{0,1},{1,0},{2,3},{3,2},{4,5},{5,4},{6,7},{7,6},{8,9},{9,8},{10,11... | collective-permute-start | bytes 393224 | tf_op jit(solution)/shard_map/ppermute | solution.py:116
  (1 other events, 1.0 us)
